TPU v7x, 32 devices: a whole 2x2x4 slice. The times are simulated.
32 devices in a mesh: ep: 8 (over z, x), tp: 4 (over y, core).
Axes of the slice: x: 2, y: 2, z: 4, core: 2. Of those that a mesh axis runs over, the one named last changes fastest.
Arguments:
- queries: bfloat16 [4096, 1024], P('ep', 'tp'), may hold values from -6 to 6
- forget_forward_logits: bfloat16 [4096, 1024], P('ep', 'tp'), may hold values from -6 to 12
- forget_backward_logits: bfloat16 [4096, 1024], P('ep', 'tp'), may hold values from -6 to 12
- values: bfloat16 [4096, 1024], P('ep', 'tp'), may hold values from -6 to 6
- output_gate_logits: bfloat16 [4096, 1024], P('ep', 'tp'), may hold values from -6 to 6
- lower_bound_forward: float32 [1024], P('tp')
- lower_bound_backward: float32 [1024], P('tp')
- extra_log_decay: float32 [4096, 8], P('ep', 'tp'), may hold values from -2 to 0
- head_norm_scale: float32 [1024], P('tp'), may hold values from 0.1 to 1.9
- output_projection: bfloat16 [1024, 2048], P('tp'), may hold values from -0.1875 to 0.1875
- second_residual: bfloat16 [4096, 2048], P('ep'), may hold values from -6 to 6
- expert_norm_scale: float32 [2048], replicated, may hold values from 0.1 to 1.9
- routes: int32 [4096, 2], P('ep'), may hold values from 0 to 7, all different within a row; in each aligned block of 128 rows (0 to 127, 128 to 255, ...) at most 64 rows name the same one
- specialist_mixing_factor: float32 [4096, 2], P(('ep', 'tp')), may hold values from 0.1 to 1
- expert_gate_matrix: bfloat16 [8, 2048, 1024], P('ep', None, 'tp'), may hold values from -0.125 to 0.125
- expert_up_matrix: bfloat16 [8, 2048, 1024], P('ep', None, 'tp'), may hold values from -0.125 to 0.125
- expert_down_matrix: bfloat16 [8, 1024, 2048], P('ep', 'tp'), may hold values from -0.1875 to 0.1875
Outputs:
- mixer_output: bfloat16 [4096, 2048], P(('ep', 'tp'))
- routed_output: bfloat16 [4096, 2048], P(('ep', 'tp'))
Inputs may be any that keep to these rules, and one draw needn't show every extreme that they name: `routes`: in each aligned block of 128 rows no expert is named by more than 64 rows; the 2 experts of a row differ.
All inputs are finite; a program needn't handle non-finite values.
Results may differ from a plain program's by a relative error of at most 0.014.
Values may be sent and summed in bfloat16 or wider, within the bound.
A program may use at most 128 MiB of HBM per device.

v0:
```python
import functools

import jax
import jax.numpy as jnp
from jax import lax
from jax.experimental import pallas as pl
from jax.experimental.pallas import tpu as pltpu
from jax.sharding import PartitionSpec as P

TOPK = 2
CHUNK = 128
LEAF = 16
DECAY_ROWS = 16
EPS = 1e-06
MESH = pl.DeviceIdType.MESH
F32 = jnp.float32
BF16 = jnp.bfloat16


def neighbours():
    place, count = lax.axis_index("tp"), lax.axis_size("tp")
    return place + 1 - 2 * lax.rem(place, 2), lax.rem(place + count // 2, count)


def greet(axis, n):
    me = lax.axis_index(axis)
    barrier = pltpu.get_barrier_semaphore()

    def one(step, carry):
        peer = lax.rem(me + step, n)
        pl.semaphore_signal(barrier, inc=1, device_id={axis: peer}, device_id_type=MESH)
        return carry

    lax.fori_loop(1, n, one, 0)


def block_copy(axis, out_ref, in_ref, send_sem, recv_sem, target, source):
    return pltpu.make_async_remote_copy(
        src_ref=out_ref.at[target],
        dst_ref=in_ref.at[source],
        send_sem=send_sem.at[target],
        recv_sem=recv_sem.at[source],
        device_id={axis: target},
        device_id_type=MESH,
    )


def start_blocks(axis, n, out_ref, in_ref, send_sem, recv_sem):
    me = lax.axis_index(axis)

    def one(step, carry):
        peer = lax.rem(me + step, n)
        block_copy(axis, out_ref, in_ref, send_sem, recv_sem, peer, me).start()
        return carry

    lax.fori_loop(1, n, one, 0)
    in_ref[me] = out_ref[me]


def finish_blocks(axis, n, out_ref, in_ref, send_sem, recv_sem):
    me = lax.axis_index(axis)

    def one(step, carry):
        peer = lax.rem(me + step, n)
        copy = block_copy(axis, out_ref, in_ref, send_sem, recv_sem, peer, peer)
        copy.wait_send()
        copy.wait_recv()
        return carry

    lax.fori_loop(1, n, one, 0)


def exchange_kernel(n, quarters, rows_ref, part_ref, back_ref, sums_ref, *sems):
    greet("ep", n)
    greet("tp", quarters)
    pl.semaphore_wait(pltpu.get_barrier_semaphore(), n + quarters - 2)
    start_blocks("ep", n, rows_ref, back_ref, *sems[:2])
    start_blocks("tp", quarters, part_ref, sums_ref, *sems[2:])
    finish_blocks("tp", quarters, part_ref, sums_ref, *sems[2:])
    finish_blocks("ep", n, rows_ref, back_ref, *sems[:2])


def exchange(blocks, partials, n, quarters):
    vmem = pl.BlockSpec(memory_space=pltpu.VMEM)
    return pl.pallas_call(
        functools.partial(exchange_kernel, n, quarters),
        out_shape=(
            jax.ShapeDtypeStruct(blocks.shape, blocks.dtype),
            jax.ShapeDtypeStruct(partials.shape, partials.dtype),
        ),
        in_specs=[vmem, vmem],
        out_specs=(vmem, vmem),
        scratch_shapes=[
            pltpu.SemaphoreType.DMA((n,)),
            pltpu.SemaphoreType.DMA((n,)),
            pltpu.SemaphoreType.DMA((quarters,)),
            pltpu.SemaphoreType.DMA((quarters,)),
        ],
        compiler_params=pltpu.CompilerParams(
            collective_id=1, has_side_effects=True, vmem_limit_bytes=32 * 2**20
        ),
        cost_estimate=pl.CostEstimate(
            flops=2 * 10**10, bytes_accessed=4 * blocks.size * 2, transcendentals=0
        ),
        name="return_rows",
    )(blocks, partials)


def dot_rows(a, b):
    return lax.dot_general(a, b, (((1,), (1,)), ((), ())), preferred_element_type=F32)


def gates(logits, bound, extra):
    shrink = jnp.exp(-logits)
    opened = 1.0 / (1.0 + shrink)
    floor_part = 1.0 / (1.0 + jnp.exp(-bound))
    complement = 1.0 / (1.0 + jnp.exp(bound))
    decay = jnp.log(floor_part + complement * opened) + extra
    return complement * (shrink * opened), decay


def referenced(total, size, place):
    blocks = total.reshape(CHUNK // size, size, total.shape[-1])
    anchor = jnp.broadcast_to(blocks[:, place : place + 1, :], blocks.shape)
    return total - anchor.reshape(total.shape)


def chunk_scores(feature, key, total, backward, rows, cols):
    scores = jnp.zeros((CHUNK, CHUNK), F32)
    size = CHUNK
    while size > LEAF:
        half = size // 2
        reach = jnp.exp(-jnp.abs(referenced(total, size, half if backward else half - 1)))
        part = dot_rows((feature * reach).astype(BF16), (key * reach).astype(BF16))
        late, early = (cols, rows) if backward else (rows, cols)
        mask = (rows // size == cols // size) & (late % size >= half) & (early % size < half)
        scores = scores + jnp.where(mask, part, 0.0)
        size = half
    spread = referenced(total, LEAF, LEAF // 2 if backward else LEAF // 2 - 1)
    part = dot_rows(
        (feature * jnp.exp(spread)).astype(BF16), (key * jnp.exp(-spread)).astype(BF16)
    )
    mask = (rows // LEAF == cols // LEAF) & ((rows <= cols) if backward else (rows >= cols))
    return scores + jnp.where(mask, part, 0.0)


def mixer_kernel(
    n,
    q_ref,
    ff_ref,
    fb_ref,
    v_ref,
    og_ref,
    lbf_ref,
    lbb_ref,
    extra_ref,
    scale_ref,
    slots_ref,
    gate_ref,
    up_ref,
    down_ref,
    hidden_ref,
    arrived_ref,
    gates_ref,
    ups_ref,
    downs_ref,
    local_ref,
    reach_ref,
    part_ref,
    fade_ref,
    state_out,
    state_in,
    slot_send,
    slot_recv,
    state_send,
    state_recv,
    weight_send,
    weight_recv,
):
    me = lax.axis_index("ep")
    row_count, width = q_ref.shape
    chunks = row_count // CHUNK
    heads = extra_ref.shape[1]
    channels = width // heads
    beside, across = neighbours()
    greet("ep", n)
    barrier = pltpu.get_barrier_semaphore()
    for peer in (beside, across):
        pl.semaphore_signal(barrier, inc=1, device_id={"tp": peer}, device_id_type=MESH)
    pl.semaphore_wait(barrier, n + 1)
    weights = ((gate_ref, gates_ref), (up_ref, ups_ref), (down_ref, downs_ref))

    def weight_copy(i, hop):
        own, held = weights[i]
        return pltpu.make_async_remote_copy(
            src_ref=held.at[1] if hop == 2 else own,
            dst_ref=held.at[hop],
            send_sem=weight_send.at[i, hop],
            recv_sem=weight_recv.at[i, hop],
            device_id={"tp": across if hop == 1 else beside},
            device_id_type=MESH,
        )

    for i in range(3):
        weight_copy(i, 1).start()
    start_blocks("ep", n, slots_ref, arrived_ref, slot_send, slot_recv)
    for i in range(3):
        weight_copy(i, 0).start()
    rows = lax.broadcasted_iota(jnp.int32, (CHUNK, CHUNK), 0)
    cols = lax.broadcasted_iota(jnp.int32, (CHUNK, CHUNK), 1)

    def local(c, carry):
        at = pl.ds(pl.multiple_of(c * CHUNK, CHUNK), CHUNK)
        for h in range(heads):
            lanes = slice(h * channels, (h + 1) * channels)
            queries = q_ref[at, lanes].astype(F32)
            feature = queries / (1.0 + jnp.exp(-queries))
            value_rows = v_ref[at, lanes]
            extra = extra_ref[at, h : h + 1]
            scores = jnp.zeros((CHUNK, CHUNK), F32)
            for way, (logit_ref, bound_ref) in enumerate(((ff_ref, lbf_ref), (fb_ref, lbb_ref))):
                key, decay = gates(logit_ref[at, lanes].astype(F32), bound_ref[:, lanes], extra)
                order = (rows <= cols) if way else (rows >= cols)
                total = jnp.dot(
                    order.astype(F32),
                    decay,
                    preferred_element_type=F32,
                    precision=lax.Precision.HIGHEST,
                )
                edge = total[0:1] if way else total[CHUNK - 1 : CHUNK]
                scores = scores + chunk_scores(feature, key, total, way == 1, rows, cols)
                reach_ref[way, h, c] = (feature * jnp.exp(total)).astype(BF16)
                faded = (key * jnp.exp(edge - total)).astype(BF16)
                part_ref[way, h, c] = lax.dot_general(
                    value_rows, faded, (((0,), (0,)), ((), ())), preferred_element_type=F32
                )
                fade_ref[way, h, c] = jnp.broadcast_to(jnp.exp(edge), (8, channels))
            local_ref[h, c] = jnp.dot(
                scores.astype(BF16), value_rows, preferred_element_type=F32
            )
        return carry

    lax.fori_loop(0, chunks, local, 0)
    for way in range(2):
        for h in range(heads):
            state = jnp.zeros(part_ref.shape[3:], F32)
            fade = jnp.ones((1, channels), F32)
            for c in range(chunks)[:: -1 if way else 1]:
                step = fade_ref[way, h, c, 0:1]
                state = state * step + part_ref[way, h, c]
                fade = fade * step
            state_out[way, h, : state.shape[0]] = state.astype(BF16)
            state_out[way, h, state.shape[0] :] = jnp.broadcast_to(
                fade, (DECAY_ROWS, channels)
            ).astype(BF16)

    def state_copy(target, source):
        way = jnp.where(target > me, 0, 1)
        return pltpu.make_async_remote_copy(
            src_ref=state_out.at[way],
            dst_ref=state_in.at[source],
            send_sem=state_send.at[target],
            recv_sem=state_recv.at[source],
            device_id={"ep": target},
            device_id_type=MESH,
        )

    def send(step, carry):
        state_copy(lax.rem(me + step, n), me).start()
        return carry

    def receive(step, carry):
        peer = lax.rem(me + step, n)
        copy = state_copy(peer, peer)
        copy.wait_send()
        copy.wait_recv()
        return carry

    lax.fori_loop(1, n, send, 0)
    weight_copy(0, 1).wait_recv()
    weight_copy(0, 2).start()
    lax.fori_loop(1, n, receive, 0)
    depth = part_ref.shape[3]
    for h in range(heads):
        for way in range(2):

            def one(hop, state, way=way, h=h):
                source = n - 1 - hop if way else hop
                step = state_in[source, h, depth : depth + DECAY_ROWS].astype(F32)[0:1]
                return state * step + state_in[source, h, :depth].astype(F32)

            ahead = n - 1 - me if way else me
            state = lax.fori_loop(0, ahead, one, jnp.zeros(part_ref.shape[3:], F32))
            for c in range(chunks)[:: -1 if way else 1]:
                local_ref[h, c] += dot_rows(reach_ref[way, h, c], state.astype(BF16))
                state = state * fade_ref[way, h, c, 0:1] + part_ref[way, h, c]
        lanes = slice(h * channels, (h + 1) * channels)
        for c in range(chunks):
            at = slice(c * CHUNK, (c + 1) * CHUNK)
            combined = local_ref[h, c]
            mean_square = jnp.mean(combined * combined, axis=-1, keepdims=True)
            gate = og_ref[at, lanes].astype(F32)
            opened = combined * lax.rsqrt(mean_square + EPS) * scale_ref[:, lanes]
            hidden_ref[at, lanes] = (opened * (gate / (1.0 + jnp.exp(-gate)))).astype(BF16)
    for i in (1, 2):
        weight_copy(i, 1).wait_recv()
        weight_copy(i, 2).start()
    finish_blocks("ep", n, slots_ref, arrived_ref, slot_send, slot_recv)
    for i in range(3):
        weight_copy(i, 1).wait_send()
        for hop in (0, 2):
            weight_copy(i, hop).wait_send()
            weight_copy(i, hop).wait_recv()


def mixer(n, queries, ff, fb, values, og, lbf, lbb, extra, scale, slots, gate, up, down):
    row_count, width = queries.shape
    heads = extra.shape[1]
    channels = width // heads
    depth = values.shape[1] // heads
    chunks = row_count // CHUNK
    vmem = pl.BlockSpec(memory_space=pltpu.VMEM)
    anywhere = pl.BlockSpec(memory_space=pl.ANY)
    state = (heads, depth + DECAY_ROWS, channels)
    return pl.pallas_call(
        functools.partial(mixer_kernel, n),
        out_shape=(
            jax.ShapeDtypeStruct(values.shape, BF16),
            jax.ShapeDtypeStruct(slots.shape, slots.dtype),
        )
        + tuple(jax.ShapeDtypeStruct((3,) + w.shape, w.dtype) for w in (gate, up, down)),
        in_specs=[vmem] * 10 + [anywhere] * 3,
        out_specs=(vmem, vmem) + (anywhere,) * 3,
        scratch_shapes=[
            pltpu.VMEM((heads, chunks, CHUNK, depth), F32),
            pltpu.VMEM((2, heads, chunks, CHUNK, channels), BF16),
            pltpu.VMEM((2, heads, chunks, depth, channels), F32),
            pltpu.VMEM((2, heads, chunks, 8, channels), F32),
            pltpu.VMEM((2,) + state, BF16),
            pltpu.VMEM((n,) + state, BF16),
            pltpu.SemaphoreType.DMA((n,)),
            pltpu.SemaphoreType.DMA((n,)),
            pltpu.SemaphoreType.DMA((n,)),
            pltpu.SemaphoreType.DMA((n,)),
            pltpu.SemaphoreType.DMA((3, 3)),
            pltpu.SemaphoreType.DMA((3, 3)),
        ],
        compiler_params=pltpu.CompilerParams(
            collective_id=0, has_side_effects=True, vmem_limit_bytes=48 * 2**20
        ),
        cost_estimate=pl.CostEstimate(
            flops=4 * 10**10, bytes_accessed=6 * 2**20, transcendentals=0
        ),
        name="mix_dispatch",
    )(
        queries,
        ff,
        fb,
        values,
        og,
        lbf.reshape(1, -1),
        lbb.reshape(1, -1),
        extra,
        scale.reshape(1, -1),
        slots,
        gate,
        up,
        down,
    )


def normalize(tensor, gain):
    widened_values = tensor.astype(F32)
    return (
        widened_values
        * lax.rsqrt(jnp.mean(widened_values * widened_values, axis=-1, keepdims=True) + EPS)
        * gain
    ).astype(BF16)


def shards(
    queries,
    forget_forward_logits,
    forget_backward_logits,
    values,
    output_gate_logits,
    lower_bound_forward,
    lower_bound_backward,
    extra_log_decay,
    head_norm_scale,
    output_projection,
    second_residual,
    expert_norm_scale,
    routes,
    specialist_mixing_factor,
    expert_gate_matrix,
    expert_up_matrix,
    expert_down_matrix,
):
    group_rows, width_model = second_residual.shape
    quarters = lax.axis_size("tp")
    experts = lax.axis_size("ep")
    row_count = group_rows // quarters
    slot_count = 2 * TOPK * row_count // experts
    quarter = lax.axis_index("tp")
    gate, up, down = expert_gate_matrix[0], expert_up_matrix[0], expert_down_matrix[0]
    own_rows = normalize(
        lax.dynamic_slice_in_dim(second_residual, quarter * row_count, row_count, 0),
        expert_norm_scale,
    )
    flat_routes = lax.dynamic_slice_in_dim(routes, quarter * row_count, row_count, 0).reshape(-1)
    expert_hits = (flat_routes[:, None] == jnp.arange(experts, dtype=jnp.int32)[None, :]).astype(
        jnp.int32
    )
    ranking = jnp.sum(jnp.cumsum(expert_hits, axis=0) * expert_hits, axis=1) - 1
    target = flat_routes * slot_count + ranking
    own_pick = (
        target[:, None] == jnp.arange(experts * slot_count, dtype=jnp.int32)[None, :]
    ).astype(BF16)
    chooser = own_pick.reshape(row_count, TOPK, -1).sum(axis=1)
    outgoing = jnp.einsum("rs,rd->sd", chooser, own_rows, preferred_element_type=F32).astype(BF16)
    mixer_hidden, arrived, gates_held, ups_held, downs_held = mixer(
        experts,
        queries,
        forget_forward_logits,
        forget_backward_logits,
        values,
        output_gate_logits,
        lower_bound_forward,
        lower_bound_backward,
        extra_log_decay,
        head_norm_scale,
        outgoing.reshape(experts, slot_count, width_model),
        gate,
        up,
        down,
    )
    partials = jnp.dot(mixer_hidden, output_projection, preferred_element_type=F32).astype(BF16)
    rows_in = arrived.reshape(-1, width_model)

    def hidden_part(gate_part, up_part):
        gated = jnp.dot(rows_in, gate_part, preferred_element_type=F32)
        lifted = jnp.dot(rows_in, up_part, preferred_element_type=F32)
        return (jax.nn.silu(gated) * lifted).astype(BF16)

    result = jnp.dot(hidden_part(gate, up), down, preferred_element_type=F32)
    rest = jnp.concatenate([hidden_part(gates_held[i], ups_held[i]) for i in range(3)], axis=1)
    result = result + jnp.dot(
        rest, downs_held.reshape(-1, width_model), preferred_element_type=F32
    )
    returned, pieces = exchange(
        result.astype(BF16).reshape(experts, slot_count, width_model),
        partials.reshape(quarters, row_count, width_model),
        experts,
        quarters,
    )
    mixer_output = jnp.sum(pieces.astype(F32), axis=0).astype(BF16)
    gathered = jnp.dot(
        own_pick, returned.reshape(-1, width_model), preferred_element_type=F32
    )
    blended = jnp.sum(
        gathered.reshape(row_count, TOPK, width_model) * specialist_mixing_factor[:, :, None],
        axis=1,
    )
    return (mixer_output, blended.astype(BF16))


def solution(mesh):
    in_specs = (
        P("ep", "tp"),
        P("ep", "tp"),
        P("ep", "tp"),
        P("ep", "tp"),
        P("ep", "tp"),
        P("tp"),
        P("tp"),
        P("ep", "tp"),
        P("tp"),
        P("tp", None),
        P("ep", None),
        P(),
        P("ep", None),
        P(("ep", "tp"), None),
        P("ep", None, "tp"),
        P("ep", None, "tp"),
        P("ep", "tp", None),
    )
    out_specs = (P(("ep", "tp"), None), P(("ep", "tp"), None))
    return jax.shard_map(shards, mesh=mesh, in_specs=in_specs, out_specs=out_specs, check_vma=False)
```

profile of v0, /device:TPU:10, one launch (start us, length us, event | category | flops | bytes accessed | tf_op | source)
XLA Modules:
  0.0 169.1 jit_solution(4752923347657719068)
XLA Ops:
  0.7 1.4 fusion.5
  2.1 0.5 add_rsqrt_fusion
  2.6 0.7 constant_dynamic-slice_fusion
  3.4 0.1 eq.65
  3.5 0.1 eq.61
  3.7 0.6 reduce-window.6
  4.3 0.2 slice_reduce_fusion
  4.6 0.1 sub.7
  4.9 0.7 multiply_add_fusion
  5.7 0.8 copy.52.extra_ref
  6.6 3.4 %convolution_convert_fusion.1 = bf16[512,2048]{1,0:T(8,128)(2,1)} fusion(bf16[128,512]{1,0:T(8,128)(2,1)S(1)} %fusion.41, f32[2048]{0:T(1024)} %param.28, f32[128]{0:T(128)} %add_rsqrt_fusion, bf16[512,2048]{1,0:T(8,128)(2,1)} %param.27, s32[]{:T(128)S(6)} %select_n.4), kind=kOutput, calls=%fused_computation.2 | convolution fusion | flops 270532608 | bytes 2761220 | tf_op jit(solution)/shard_map/rs,rd->sd/dot_general | solution.py:421
  10.1 0.9 copy-done.10
  11.0 0.9 copy-done.11
  12.0 78.0 %mix_dispatch.1 = (bf16[512,256]{1,0:T(8,128)(2,1)S(1)}, bf16[8,64,2048]{2,1,0:T(8,128)(2,1)}, bf16[3,2048,256]{2,1,0:T(8,128)(2,1)}, bf16[3,2048,256]{2,1,0:T(8,128)(2,1)}, bf16[3,256,2048]{2,1,0:T(8,128)(2,1)}) custom-call(bf16[512,256]{1,0:T(8,128)(2,1)S(1)} %copy-done.7, bf16[512,256]{1,0:T(8,128)(2,1)S(1)} %copy-done.8, bf16[512,256]{1,0:T(8,128)(2,1)S(1)} %copy-done.9, ...), custom_call_target="tpu_custom_call" | custom-call | flops 40000000000 | bytes 6291456 | tf_op jit(solution)/shard_map/mix_dispatch/pallas_call | solution.py:325
  90.0 2.7 %fusion.9 = f32[512,256]{1,0:T(8,128)S(1)} fusion(bf16[512,2048]{1,0:T(8,128)(2,1)} %bitcast.71, bf16[3,2048,256]{2,1,0:T(8,128)(2,1)} %get-tuple-element.10), kind=kOutput, calls=%fused_computation.19 | convolution fusion | flops 536870912 | bytes 3670016 | tf_op jit(solution)/shard_map/dot_general | solution.py:442
  92.8 0.8 copy-done.20
  93.6 0.7 fusion.4
  94.3 1.2 copy-done.19
  95.4 0.7 fusion.12
  96.2 0.7 fusion.15
  96.9 0.7 fusion.2
  97.7 0.7 fusion.3
  98.4 1.2 copy-done.18
  99.5 3.7 %fusion.23 = f32[512,2048]{1,0:T(8,128)} fusion(bf16[768,2048]{1,0:T(8,128)(2,1)S(1)} %bitcast.79, bf16[512,256]{1,0:T(8,128)(2,1)S(1)} %fusion.4, bf16[512,256]{1,0:T(8,128)(2,1)S(1)} %fusion.3, bf16[512,256]{1,0:T(8,128)(2,1)S(1)} %fusion.2), kind=kOutput, calls=%fused_computation.33 | convolution fusion | flops 1612972032 | bytes 8126464 | tf_op jit(solution)/shard_map/dot_general | solution.py:448
  103.3 1.5 fusion.51
  104.8 6.7 %add_convert_fusion = bf16[512,2048]{1,0:T(8,128)(2,1)} fusion(f32[512,2048]{1,0:T(8,128)} %fusion.23, bf16[512,2048]{1,0:T(8,128)(2,1)} %bitcast.72, f32[512,256]{1,0:T(8,128)} %fusion.51, bf16[1,256,2048]{2,1,0:T(8,128)(2,1)S(1)} %copy-done.3, bf16[1,2048,256]{2,1,0:T(8,128)(2,1)S(1)} %copy-done.2), kind=kOutput, calls=%fused_computation | convolution fusion | flops 1076625408 | bytes 11010048 | tf_op jit(solution)/shard_map/dot_general | solution.py:446
  111.5 0.7 convolution_convert_fusion
  112.2 0.9 copy-done.1
  113.1 50.0 %return_rows.1 = (bf16[8,64,2048]{2,1,0:T(8,128)(2,1)S(1)}, bf16[4,128,2048]{2,1,0:T(8,128)(2,1)S(1)}) custom-call(bf16[8,64,2048]{2,1,0:T(8,128)(2,1)S(1)} %bitcast.62, bf16[4,128,2048]{2,1,0:T(8,128)(2,1)S(1)} %bitcast.61), custom_call_target="tpu_custom_call" | custom-call | flops 20000000000 | bytes 8388608 | tf_op jit(solution)/shard_map/return_rows/pallas_call | solution.py:85
  163.1 1.3 copy-done.15
  164.4 1.3 reduce_sum.54
  165.8 3.3 %fusion = bf16[128,2048]{1,0:T(8,128)(2,1)} fusion(bf16[512,2048,1]{1,0,2:T(8,128)(2,1)} %bitcast.69, f32[128,2]{0,1:T(2,128)S(1)} %copy-done.17, s32[128,2]{0,1:T(2,128)S(1)} %multiply_add_fusion), kind=kOutput, calls=%fused_computation.4 | convolution fusion | flops 537788416 | bytes 2623488 | tf_op jit(solution)/shard_map/dot_general | solution.py:458
  (43 shorter events, 0.5 us)
Async XLA Ops:
  0.6 110.8 %copy-start = (bf16[256,2048]{1,0:T(8,128)(2,1)S(1)}, bf16[256,2048]{1,0:T(8,128)(2,1)}, u32[]{:S(2)}) copy-start(bf16[256,2048]{1,0:T(8,128)(2,1)} %param.26) | copy-start | bytes 3145732
  0.6 9.4 %copy-start.3 = (bf16[1,256,2048]{2,1,0:T(8,128)(2,1)S(1)}, bf16[1,256,2048]{2,1,0:T(8,128)(2,1)}, u32[]{:S(2)}) copy-start(bf16[1,256,2048]{2,1,0:T(8,128)(2,1)} %param.33) | copy-start | bytes 3145732
  0.7 9.3 %copy-start.2 = (bf16[1,2048,256]{2,1,0:T(8,128)(2,1)S(1)}, bf16[1,2048,256]{2,1,0:T(8,128)(2,1)}, u32[]{:S(2)}) copy-start(bf16[1,2048,256]{2,1,0:T(8,128)(2,1)} %param.32) | copy-start | bytes 3145732
  0.7 9.3 %copy-start.14 = (f32[256]{0:T(256)S(1)}, f32[256]{0:T(256)}, u32[]{:S(2)}) copy-start(f32[256]{0:T(256)} %param.25) | copy-start | bytes 3076
  0.7 9.3 %copy-start.13 = (f32[256]{0:T(256)S(1)}, f32[256]{0:T(256)}, u32[]{:S(2)}) copy-start(f32[256]{0:T(256)} %param.23) | copy-start | bytes 3076
  0.7 9.3 %copy-start.12 = (f32[256]{0:T(256)S(1)}, f32[256]{0:T(256)}, u32[]{:S(2)}) copy-start(f32[256]{0:T(256)} %param.22) | copy-start | bytes 3076
  6.5 3.5 %copy-start.6 = (bf16[1,2048,256]{2,1,0:T(8,128)(2,1)S(1)}, bf16[1,2048,256]{2,1,0:T(8,128)(2,1)}, u32[]{:S(2)}) copy-start(bf16[1,2048,256]{2,1,0:T(8,128)(2,1)} %param.31) | copy-start | bytes 3145732
  6.5 3.5 %copy-start.7 = (bf16[512,256]{1,0:T(8,128)(2,1)S(1)}, bf16[512,256]{1,0:T(8,128)(2,1)}, u32[]{:S(2)}) copy-start(bf16[512,256]{1,0:T(8,128)(2,1)} %q_ref.1) | copy-start | bytes 786436
  6.5 3.5 %copy-start.8 = (bf16[512,256]{1,0:T(8,128)(2,1)S(1)}, bf16[512,256]{1,0:T(8,128)(2,1)}, u32[]{:S(2)}) copy-start(bf16[512,256]{1,0:T(8,128)(2,1)} %ff_ref.1) | copy-start | bytes 786436
  6.6 3.5 %copy-start.9 = (bf16[512,256]{1,0:T(8,128)(2,1)S(1)}, bf16[512,256]{1,0:T(8,128)(2,1)}, u32[]{:S(2)}) copy-start(bf16[512,256]{1,0:T(8,128)(2,1)} %fb_ref.1) | copy-start | bytes 786436
  10.1 1.0 copy-start.10
  11.0 0.9 copy-start.11
  90.0 2.8 %copy-start.4 = (bf16[512,256]{1,0:T(8,128)(2,1)}, bf16[512,256]{1,0:T(8,128)(2,1)S(1)}, u32[]{:S(2)}) copy-start(bf16[512,256]{1,0:T(8,128)(2,1)S(1)} %get-tuple-element.13) | copy-start | bytes 786436
  90.0 2.8 %copy-start.16 = (bf16[8,64,2048]{2,1,0:T(8,128)(2,1)S(1)}, bf16[8,64,2048]{2,1,0:T(8,128)(2,1)}, u32[]{:S(2)}) copy-start(bf16[8,64,2048]{2,1,0:T(8,128)(2,1)} %get-tuple-element.9) | copy-start | bytes 6291460
  90.0 3.6 %copy-start.20 = (bf16[3,2048,256]{2,1,0:T(8,128)(2,1)S(1)}, bf16[3,2048,256]{2,1,0:T(8,128)(2,1)}, u32[]{:S(2)}) copy-start(bf16[3,2048,256]{2,1,0:T(8,128)(2,1)} %get-tuple-element.11) | copy-start | bytes 9437188
  93.6 1.9 %copy-start.19 = (bf16[3,2048,256]{2,1,0:T(8,128)(2,1)S(1)}, bf16[3,2048,256]{2,1,0:T(8,128)(2,1)}, u32[]{:S(2)}) copy-start(bf16[3,2048,256]{2,1,0:T(8,128)(2,1)} %get-tuple-element.10) | copy-start | bytes 9437188
  97.7 1.9 %copy-start.18 = (bf16[3,256,2048]{2,1,0:T(8,128)(2,1)S(1)}, bf16[3,256,2048]{2,1,0:T(8,128)(2,1)}, u32[]{:S(2)}) copy-start(bf16[3,256,2048]{2,1,0:T(8,128)(2,1)} %get-tuple-element.12) | copy-start | bytes 9437188
  104.8 6.7 %copy-start.5 = (bf16[512,256]{1,0:T(8,128)(2,1)S(1)}, bf16[512,256]{1,0:T(8,128)(2,1)}, u32[]{:S(2)}) copy-start(bf16[512,256]{1,0:T(8,128)(2,1)} %copy-done.4) | copy-start | bytes 786436
  111.5 1.6 copy-start.1
  163.1 1.4 copy-start.15
  164.4 1.3 copy-start.17
where the time goes:
time: 170 us; the launch traced here: 169 us
  Pallas kernels  128 us (75%)
  matrix products  25.7 us (15%)
  local copies, waits for them, and re-layouts  9.6 us (6%)
  other arithmetic  4.76 us (3%)
    pallas_call x1, Pallas kernels, mixer(): pl.pallas_call(functools.partial(mixer_kernel, n), out_shape=(jax.ShapeDt...  78 us
    pallas_call x1, Pallas kernels, exchange(): pl.pallas_call(functools.partial(exchange_kernel, n, quarters), out_shape...  50 us
    unnamed x43, local copies, waits for them, and re-layouts  8.11 us
    dot_general x1, matrix products, shards(): result = jnp.dot(hidden_part(gate, up), down, preferred_element_type=F32)  6.67 us
    dot_general x4, matrix products, hidden_part(): gated = jnp.dot(rows_in, gate_part, preferred_element_type=F32)  5.7 us
    dot_general x1, matrix products, shards(): jnp.dot(rest, downs_held.reshape(-1, width_model), preferred_element_type...  3.72 us
    dot_general x1, matrix products, shards(): jnp.einsum('rs,rd->sd', chooser, own_rows, preferred_element_type=F32)  3.43 us

commit v1 on v0

v1 whole, which is shorter than its diff:
```python
import functools

import jax
import jax.numpy as jnp
from jax import lax
from jax.experimental import pallas as pl
from jax.experimental.pallas import tpu as pltpu
from jax.sharding import PartitionSpec as P

TOPK = 2
CHUNK = 128
LEAF = 16
DECAY_ROWS = 16
PIECES = 4
EPS = 1e-06
MESH = pl.DeviceIdType.MESH
F32 = jnp.float32
BF16 = jnp.bfloat16


def neighbours():
    place, count = lax.axis_index("tp"), lax.axis_size("tp")
    return place + 1 - 2 * lax.rem(place, 2), lax.rem(place + count // 2, count)


def greet(axis, n):
    me = lax.axis_index(axis)
    barrier = pltpu.get_barrier_semaphore()

    def one(step, carry):
        peer = lax.rem(me + step, n)
        pl.semaphore_signal(barrier, inc=1, device_id={axis: peer}, device_id_type=MESH)
        return carry

    lax.fori_loop(1, n, one, 0)


def dot_rows(a, b):
    return lax.dot_general(a, b, (((1,), (1,)), ((), ())), preferred_element_type=F32)


def gates(logits, bound, extra):
    shrink = jnp.exp(-logits)
    opened = 1.0 / (1.0 + shrink)
    floor_part = 1.0 / (1.0 + jnp.exp(-bound))
    complement = 1.0 / (1.0 + jnp.exp(bound))
    decay = jnp.log(floor_part + complement * opened) + extra
    return complement * (shrink * opened), decay


def referenced(total, size, place):
    blocks = total.reshape(CHUNK // size, size, total.shape[-1])
    anchor = jnp.broadcast_to(blocks[:, place : place + 1, :], blocks.shape)
    return total - anchor.reshape(total.shape)


def chunk_scores(feature, key, total, backward, rows, cols):
    scores = jnp.zeros((CHUNK, CHUNK), F32)
    size = CHUNK
    while size > LEAF:
        half = size // 2
        reach = jnp.exp(-jnp.abs(referenced(total, size, half if backward else half - 1)))
        part = dot_rows((feature * reach).astype(BF16), (key * reach).astype(BF16))
        late, early = (cols, rows) if backward else (rows, cols)
        mask = (rows // size == cols // size) & (late % size >= half) & (early % size < half)
        scores = scores + jnp.where(mask, part, 0.0)
        size = half
    spread = referenced(total, LEAF, LEAF // 2 if backward else LEAF // 2 - 1)
    part = dot_rows(
        (feature * jnp.exp(spread)).astype(BF16), (key * jnp.exp(-spread)).astype(BF16)
    )
    mask = (rows // LEAF == cols // LEAF) & ((rows <= cols) if backward else (rows >= cols))
    return scores + jnp.where(mask, part, 0.0)


def fused_kernel(
    n,
    quarters,
    q_any,
    ff_any,
    fb_any,
    v_any,
    og_any,
    lbf_ref,
    lbb_ref,
    extra_ref,
    scale_ref,
    proj_any,
    resid_any,
    gain_ref,
    routes_ref,
    mix_ref,
    gate_any,
    up_any,
    down_any,
    mixed_ref,
    routed_ref,
    q_ref,
    ff_ref,
    fb_ref,
    v_ref,
    og_ref,
    proj_ref,
    resid_ref,
    ranks_ref,
    shares_ref,
    chooser_ref,
    blend_ref,
    slots_ref,
    arrived_ref,
    gates_ref,
    ups_ref,
    downs_ref,
    active_ref,
    leaving_ref,
    returned_ref,
    local_ref,
    reach_ref,
    part_ref,
    fade_ref,
    state_out,
    state_in,
    hidden_ref,
    partial_ref,
    pieces_ref,
    load_sem,
    slot_send,
    slot_recv,
    state_send,
    state_recv,
    weight_send,
    weight_recv,
    back_send,
    back_recv,
    piece_send,
    piece_recv,
):
    me = lax.axis_index("ep")
    place = lax.axis_index("tp")
    group_rows, width = q_ref.shape
    row_count, width_model = resid_ref.shape
    chunks = group_rows // CHUNK
    heads = extra_ref.shape[0]
    channels = width // heads
    slot_total = slots_ref.shape[0]
    slot_count = slot_total // n
    pieces, _, span = leaving_ref.shape
    units = down_any.shape[1]
    beside, across = neighbours()

    first_row = pl.multiple_of(place * row_count, row_count)
    loads = [
        pltpu.make_async_copy(source, target, load_sem.at[i])
        for i, (source, target) in enumerate(
            (
                (resid_any.at[pl.ds(first_row, row_count)], resid_ref),
                (q_any, q_ref),
                (ff_any, ff_ref),
                (fb_any, fb_ref),
                (v_any, v_ref),
                (og_any, og_ref),
                (proj_any, proj_ref),
                (gate_any.at[0], gates_ref.at[3]),
                (up_any.at[0], ups_ref.at[3]),
            )
            + tuple(
                (
                    down_any.at[0, :, c * span : (c + 1) * span],
                    downs_ref.at[c, 3 * units : 4 * units],
                )
                for c in range(pieces)
            )
        )
    ]
    for load in loads:
        load.start()

    greet("ep", n)
    greet("tp", quarters)
    pl.semaphore_wait(pltpu.get_barrier_semaphore(), n + quarters - 2)

    def weight_copy(i, hop):
        if i < 2:
            own, held = ((gate_any.at[0], gates_ref), (up_any.at[0], ups_ref))[i]
            target, passed = held.at[hop], held.at[1]
        else:
            c = i - 2
            own = down_any.at[0, :, c * span : (c + 1) * span]
            target = downs_ref.at[c, hop * units : (hop + 1) * units]
            passed = downs_ref.at[c, units : 2 * units]
        return pltpu.make_async_remote_copy(
            src_ref=passed if hop == 2 else own,
            dst_ref=target,
            send_sem=weight_send.at[i, hop],
            recv_sem=weight_recv.at[i, hop],
            device_id={"tp": across if hop == 1 else beside},
            device_id_type=MESH,
        )

    for i in range(2 + pieces):
        weight_copy(i, 1).start()

    lanes = pl.ds(first_row, row_count)
    expert = lax.broadcasted_iota(jnp.int32, (n, row_count), 0)
    hits = jnp.zeros((n, row_count), F32)
    shares = jnp.zeros((n, row_count), F32)
    for k in range(TOPK):
        chosen = routes_ref[k : k + 1, lanes] == expert
        hits = jnp.where(chosen, 1.0, hits)
        shares = jnp.where(chosen, mix_ref[k : k + 1], shares)
    before = lax.broadcasted_iota(jnp.int32, (row_count, row_count), 0)
    after = lax.broadcasted_iota(jnp.int32, (row_count, row_count), 1)
    earlier = (before < after).astype(BF16)
    ranks = jnp.dot(hits.astype(BF16), earlier, preferred_element_type=F32)
    ranks_ref[...] = jnp.where(hits > 0.0, ranks, -1.0)
    shares_ref[...] = shares
    slot = lax.broadcasted_iota(jnp.int32, (slot_count, row_count), 0).astype(F32)
    picks, blends = [], []
    for e in range(n):
        match = slot == ranks_ref[e : e + 1]
        picks.append(jnp.where(match, 1.0, 0.0))
        blends.append(jnp.where(match, shares_ref[e : e + 1], 0.0))
    chooser_ref[...] = jnp.concatenate(picks, axis=0).astype(BF16)

    loads[0].wait()
    rows_wide = resid_ref[...].astype(F32)
    mean_square = jnp.mean(rows_wide * rows_wide, axis=-1, keepdims=True)
    own_rows = (rows_wide * lax.rsqrt(mean_square + EPS) * gain_ref[...]).astype(BF16)
    for g in range(slot_total // row_count):
        at = slice(g * row_count, (g + 1) * row_count)
        slots_ref[at] = jnp.dot(
            chooser_ref[at], own_rows, preferred_element_type=F32
        ).astype(BF16)

    def block(ref, index):
        return ref.at[pl.ds(pl.multiple_of(index * slot_count, slot_count), slot_count)]

    def slot_copy(target, source):
        return pltpu.make_async_remote_copy(
            src_ref=block(slots_ref, target),
            dst_ref=block(arrived_ref, source),
            send_sem=slot_send.at[target],
            recv_sem=slot_recv.at[source],
            device_id={"ep": target},
            device_id_type=MESH,
        )

    def back_copy(c, target, source):
        return pltpu.make_async_remote_copy(
            src_ref=block(leaving_ref.at[c], target),
            dst_ref=block(returned_ref.at[c], source),
            send_sem=back_send.at[c, target],
            recv_sem=back_recv.at[c, source],
            device_id={"ep": target},
            device_id_type=MESH,
        )

    def each_peer(act):
        def one(step, carry):
            act(lax.rem(me + step, n))
            return carry

        lax.fori_loop(1, n, one, 0)

    each_peer(lambda peer: slot_copy(peer, me).start())
    for i in range(2 + pieces):
        weight_copy(i, 0).start()
    here = pl.ds(pl.multiple_of(me * slot_count, slot_count), slot_count)
    arrived_ref[here] = slots_ref[here]
    blend = jnp.concatenate(blends, axis=0).T
    blend_high = blend.astype(BF16)
    blend_ref[0] = blend_high
    blend_ref[1] = (blend - blend_high.astype(F32)).astype(BF16)

    for load in loads[1:6]:
        load.wait()
    rows = lax.broadcasted_iota(jnp.int32, (CHUNK, CHUNK), 0)
    cols = lax.broadcasted_iota(jnp.int32, (CHUNK, CHUNK), 1)

    def local(c, carry):
        at = pl.ds(pl.multiple_of(c * CHUNK, CHUNK), CHUNK)
        for h in range(heads):
            lanes = slice(h * channels, (h + 1) * channels)
            queries = q_ref[at, lanes].astype(F32)
            feature = queries / (1.0 + jnp.exp(-queries))
            value_rows = v_ref[at, lanes]
            extra = jnp.broadcast_to(extra_ref[h : h + 1, at], (channels, CHUNK)).T
            scores = jnp.zeros((CHUNK, CHUNK), F32)
            for way, (logit_ref, bound_ref) in enumerate(((ff_ref, lbf_ref), (fb_ref, lbb_ref))):
                key, decay = gates(logit_ref[at, lanes].astype(F32), bound_ref[:, lanes], extra)
                order = (rows <= cols) if way else (rows >= cols)
                total = jnp.dot(
                    order.astype(F32),
                    decay,
                    preferred_element_type=F32,
                    precision=lax.Precision.HIGHEST,
                )
                edge = total[0:1] if way else total[CHUNK - 1 : CHUNK]
                scores = scores + chunk_scores(feature, key, total, way == 1, rows, cols)
                reach_ref[way, h, c] = (feature * jnp.exp(total)).astype(BF16)
                faded = (key * jnp.exp(edge - total)).astype(BF16)
                part_ref[way, h, c] = lax.dot_general(
                    value_rows, faded, (((0,), (0,)), ((), ())), preferred_element_type=F32
                )
                fade_ref[way, h, c] = jnp.broadcast_to(jnp.exp(edge), (8, channels))
            local_ref[h, c] = jnp.dot(
                scores.astype(BF16), value_rows, preferred_element_type=F32
            )
        return carry

    lax.fori_loop(0, chunks, local, 0)
    for way in range(2):
        for h in range(heads):
            state = jnp.zeros(part_ref.shape[3:], F32)
            fade = jnp.ones((1, channels), F32)
            for c in range(chunks)[:: -1 if way else 1]:
                step = fade_ref[way, h, c, 0:1]
                state = state * step + part_ref[way, h, c]
                fade = fade * step
            state_out[way, h, : state.shape[0]] = state.astype(BF16)
            state_out[way, h, state.shape[0] :] = jnp.broadcast_to(
                fade, (DECAY_ROWS, channels)
            ).astype(BF16)

    def state_copy(target, source):
        way = jnp.where(target > me, 0, 1)
        return pltpu.make_async_remote_copy(
            src_ref=state_out.at[way],
            dst_ref=state_in.at[source],
            send_sem=state_send.at[target],
            recv_sem=state_recv.at[source],
            device_id={"ep": target},
            device_id_type=MESH,
        )

    each_peer(lambda peer: state_copy(peer, me).start())

    def activate(i):
        arrived = arrived_ref[...]
        gated = jnp.dot(arrived, gates_ref[i], preferred_element_type=F32)
        lifted = jnp.dot(arrived, ups_ref[i], preferred_element_type=F32)
        active_ref[:, i * units : (i + 1) * units] = (
            gated / (1.0 + jnp.exp(-gated)) * lifted
        ).astype(BF16)

    for load in loads[6:]:
        load.wait()
    for i in range(2 + pieces):
        weight_copy(i, 0).wait_recv()
    weight_copy(0, 1).wait_recv()
    weight_copy(0, 2).start()
    each_peer(lambda peer: slot_copy(peer, peer).wait_recv())
    activate(3)
    activate(0)
    weight_copy(1, 1).wait_recv()
    weight_copy(1, 2).start()
    activate(1)
    weight_copy(0, 2).wait_recv()
    weight_copy(1, 2).wait_recv()
    activate(2)

    def results(c):
        weight_copy(2 + c, 1).wait_recv()
        weight_copy(2 + c, 2).start()
        weight_copy(2 + c, 2).wait_recv()
        leaving_ref[c] = jnp.dot(
            active_ref[...], downs_ref[c], preferred_element_type=F32
        ).astype(BF16)
        each_peer(lambda peer: back_copy(c, peer, me).start())
        returned_ref[c, here] = leaving_ref[c, here]

    def collect(c):
        each_peer(lambda peer: back_copy(c, peer, peer).wait_recv())
        came = returned_ref[c]
        total = jnp.dot(blend_ref[0], came, preferred_element_type=F32)
        total = total + jnp.dot(blend_ref[1], came, preferred_element_type=F32)
        routed_ref[:, c * span : (c + 1) * span] = total.astype(BF16)

    def finish_mixer():
        each_peer(lambda peer: state_copy(peer, peer).wait_recv())
        depth = part_ref.shape[3]
        for h in range(heads):
            for way in range(2):

                def one(hop, state, way=way, h=h):
                    source = n - 1 - hop if way else hop
                    step = state_in[source, h, depth : depth + DECAY_ROWS].astype(F32)[0:1]
                    return state * step + state_in[source, h, :depth].astype(F32)

                ahead = n - 1 - me if way else me
                state = lax.fori_loop(0, ahead, one, jnp.zeros(part_ref.shape[3:], F32))
                for c in range(chunks)[:: -1 if way else 1]:
                    local_ref[h, c] += dot_rows(reach_ref[way, h, c], state.astype(BF16))
                    state = state * fade_ref[way, h, c, 0:1] + part_ref[way, h, c]
            lanes = slice(h * channels, (h + 1) * channels)
            for c in range(chunks):
                at = slice(c * CHUNK, (c + 1) * CHUNK)
                combined = local_ref[h, c]
                mean_square = jnp.mean(combined * combined, axis=-1, keepdims=True)
                gate = og_ref[at, lanes].astype(F32)
                opened = combined * lax.rsqrt(mean_square + EPS) * scale_ref[:, lanes]
                hidden_ref[at, lanes] = (opened * (gate / (1.0 + jnp.exp(-gate)))).astype(BF16)

    def piece_copy(target, source):
        return pltpu.make_async_remote_copy(
            src_ref=partial_ref.at[target],
            dst_ref=pieces_ref.at[source],
            send_sem=piece_send.at[target],
            recv_sem=piece_recv.at[source],
            device_id={"tp": target},
            device_id_type=MESH,
        )

    def each_part(act):
        def one(step, carry):
            act(lax.rem(place + step, quarters))
            return carry

        lax.fori_loop(1, quarters, one, 0)

    def project():
        for part in range(quarters):
            at = slice(part * row_count, (part + 1) * row_count)
            partial_ref[part] = jnp.dot(
                hidden_ref[at], proj_ref[...], preferred_element_type=F32
            ).astype(BF16)
        each_part(lambda peer: piece_copy(peer, place).start())
        pieces_ref[place] = partial_ref[place]

    def gather_mixed():
        each_part(lambda peer: piece_copy(peer, peer).wait_recv())
        total = pieces_ref[0].astype(F32)
        for part in range(1, quarters):
            total = total + pieces_ref[part].astype(F32)
        mixed_ref[...] = total.astype(BF16)

    results(0)
    finish_mixer()
    results(1)
    project()
    for c in range(2, pieces):
        results(c)
    for c in range(pieces - 1):
        collect(c)
    gather_mixed()
    collect(pieces - 1)

    each_peer(lambda peer: slot_copy(peer, peer).wait_send())
    each_peer(lambda peer: state_copy(peer, peer).wait_send())
    for c in range(pieces):
        each_peer(lambda peer, c=c: back_copy(c, peer, peer).wait_send())
    each_part(lambda peer: piece_copy(peer, peer).wait_send())
    for i in range(2 + pieces):
        for hop in range(3):
            weight_copy(i, hop).wait_send()


def shards(
    queries,
    forget_forward_logits,
    forget_backward_logits,
    values,
    output_gate_logits,
    lower_bound_forward,
    lower_bound_backward,
    extra_log_decay,
    head_norm_scale,
    output_projection,
    second_residual,
    expert_norm_scale,
    routes,
    specialist_mixing_factor,
    expert_gate_matrix,
    expert_up_matrix,
    expert_down_matrix,
):
    group_rows, width_model = second_residual.shape
    quarters = lax.axis_size("tp")
    n = lax.axis_size("ep")
    row_count = group_rows // quarters
    slot_count = 2 * TOPK * row_count // n
    slot_total = n * slot_count
    width = queries.shape[1]
    heads = extra_log_decay.shape[1]
    channels = width // heads
    depth = values.shape[1] // heads
    chunks = group_rows // CHUNK
    units = expert_down_matrix.shape[1]
    span = width_model // PIECES
    vmem = pl.BlockSpec(memory_space=pltpu.VMEM)
    anywhere = pl.BlockSpec(memory_space=pl.ANY)
    state = (heads, depth + DECAY_ROWS, channels)
    block = (group_rows, width)
    out = jax.ShapeDtypeStruct((row_count, width_model), BF16)
    dma = pltpu.SemaphoreType.DMA
    return pl.pallas_call(
        functools.partial(fused_kernel, n, quarters),
        out_shape=(out, out),
        in_specs=[anywhere] * 5
        + [vmem] * 4
        + [anywhere] * 2
        + [vmem] * 3
        + [anywhere] * 3,
        out_specs=(vmem, vmem),
        scratch_shapes=[pltpu.VMEM(block, BF16)] * 5
        + [
            pltpu.VMEM((width, width_model), BF16),
            pltpu.VMEM((row_count, width_model), BF16),
            pltpu.VMEM((n, row_count), F32),
            pltpu.VMEM((n, row_count), F32),
            pltpu.VMEM((slot_total, row_count), BF16),
            pltpu.VMEM((2, row_count, slot_total), BF16),
            pltpu.VMEM((slot_total, width_model), BF16),
            pltpu.VMEM((slot_total, width_model), BF16),
            pltpu.VMEM((quarters,) + expert_gate_matrix.shape[1:], BF16),
            pltpu.VMEM((quarters,) + expert_up_matrix.shape[1:], BF16),
            pltpu.VMEM((PIECES, quarters * units, span), BF16),
            pltpu.VMEM((slot_total, quarters * units), BF16),
            pltpu.VMEM((PIECES, slot_total, span), BF16),
            pltpu.VMEM((PIECES, slot_total, span), BF16),
            pltpu.VMEM((heads, chunks, CHUNK, depth), F32),
            pltpu.VMEM((2, heads, chunks, CHUNK, channels), BF16),
            pltpu.VMEM((2, heads, chunks, depth, channels), F32),
            pltpu.VMEM((2, heads, chunks, 8, channels), F32),
            pltpu.VMEM((2,) + state, BF16),
            pltpu.VMEM((n,) + state, BF16),
            pltpu.VMEM(block, BF16),
            pltpu.VMEM((quarters, row_count, width_model), BF16),
            pltpu.VMEM((quarters, row_count, width_model), BF16),
            dma((9 + PIECES,)),
            dma((n,)),
            dma((n,)),
            dma((n,)),
            dma((n,)),
            dma((2 + PIECES, 3)),
            dma((2 + PIECES, 3)),
            dma((PIECES, n)),
            dma((PIECES, n)),
            dma((quarters,)),
            dma((quarters,)),
        ],
        compiler_params=pltpu.CompilerParams(
            collective_id=0, has_side_effects=True, vmem_limit_bytes=60 * 2**20
        ),
        cost_estimate=pl.CostEstimate(
            flops=4 * 10**10, bytes_accessed=30 * 2**20, transcendentals=0
        ),
        name="mix_and_route",
    )(
        queries,
        forget_forward_logits,
        forget_backward_logits,
        values,
        output_gate_logits,
        lower_bound_forward.reshape(1, -1),
        lower_bound_backward.reshape(1, -1),
        extra_log_decay.T,
        head_norm_scale.reshape(1, -1),
        output_projection,
        second_residual,
        expert_norm_scale.reshape(1, -1),
        routes.T,
        specialist_mixing_factor.T,
        expert_gate_matrix,
        expert_up_matrix,
        expert_down_matrix,
    )


def solution(mesh):
    in_specs = (
        P("ep", "tp"),
        P("ep", "tp"),
        P("ep", "tp"),
        P("ep", "tp"),
        P("ep", "tp"),
        P("tp"),
        P("tp"),
        P("ep", "tp"),
        P("tp"),
        P("tp", None),
        P("ep", None),
        P(),
        P("ep", None),
        P(("ep", "tp"), None),
        P("ep", None, "tp"),
        P("ep", None, "tp"),
        P("ep", "tp", None),
    )
    out_specs = (P(("ep", "tp"), None), P(("ep", "tp"), None))
    return jax.shard_map(shards, mesh=mesh, in_specs=in_specs, out_specs=out_specs, check_vma=False)
```

time: 170 us -> 117 us (0.69)
  the two profiles are of different devices: /device:TPU:10 before, /device:TPU:0 now
where the time goes in v1:
time: 117 us; the launch traced here: 116 us
  Pallas kernels  112 us (96%)
  local copies, waits for them, and re-layouts  3.76 us (3%)
    pallas_call x1, Pallas kernels, shards(): pl.pallas_call(functools.partial(fused_kernel, n, quarters), out_shape=(o...  112 us
    unnamed x2, local copies, waits for them, and re-layouts  3.76 us

profile of v1, /device:TPU:0, one launch (start us, length us, event | category | flops | bytes accessed | tf_op | source)
XLA Modules:
  0.0 116.1 jit_solution(6119706211885125708)
XLA Ops:
  0.6 111.7 %mix_and_route.1 = (bf16[128,2048]{1,0:T(8,128)(2,1)}, bf16[128,2048]{1,0:T(8,128)(2,1)}) custom-call(bf16[512,256]{1,0:T(8,128)(2,1)} %q_any.1, bf16[512,256]{1,0:T(8,128)(2,1)} %ff_any.1, bf16[512,256]{1,0:T(8,128)(2,1)} %fb_any.1, bf16[512,256]{1,0:T(8,128)(2,1)} %v_any.1, bf16[512,256]{1,0:T(8,128)(2,1)} %og_any.1, f32[1,256]{1,0:T(1,128)} %bitcast.10, ...), custom_call_target="tpu_custom_call" | custom-call | flops 40000000000 | bytes 31457280 | tf_op jit(solution)/shard_map/mix_and_route/pallas_call | solution.py:496
  112.3 1.9 %copy.21 = bf16[128,2048]{1,0:T(8,128)(2,1)} copy(bf16[128,2048]{1,0:T(8,128)(2,1)} %get-tuple-element.4) | data formatting | bytes 1048576
  114.2 1.9 %copy.22 = bf16[128,2048]{1,0:T(8,128)(2,1)} copy(bf16[128,2048]{1,0:T(8,128)(2,1)} %get-tuple-element.5) | data formatting | bytes 1048576

commit v2 on v1

--- a/solution.py
+++ b/solution.py
@@ -11,7 +11,8 @@
 CHUNK = 128
 LEAF = 16
 DECAY_ROWS = 16
-PIECES = 4
+PIECES = 8
+PLANES = 4
 EPS = 1e-06
 MESH = pl.DeviceIdType.MESH
 F32 = jnp.float32
@@ -102,18 +103,26 @@
     og_ref,
     proj_ref,
     resid_ref,
-    ranks_ref,
-    shares_ref,
+    meta_ref,
+    meta_in,
+    rows_ref,
+    rows_in,
     chooser_ref,
     blend_ref,
+    merge_blend,
     slots_ref,
     arrived_ref,
+    passed_ref,
     gates_ref,
     ups_ref,
     downs_ref,
     active_ref,
     leaving_ref,
     returned_ref,
+    merge_in,
+    merged_ref,
+    merged_in,
+    total_ref,
     local_ref,
     reach_ref,
     part_ref,
@@ -122,8 +131,15 @@
     state_in,
     hidden_ref,
     partial_ref,
+    summed_ref,
     pieces_ref,
     load_sem,
+    rows_sem,
+    pass_send,
+    merge_send,
+    merge_recv,
+    merged_send,
+    merged_recv,
     slot_send,
     slot_recv,
     state_send,
@@ -148,6 +164,29 @@
     units = down_any.shape[1]
     beside, across = neighbours()
 
+    half = n // 2
+    side = half * slot_count
+    relayed = half == PLANES
+    base = me // half * half
+    other = half - base
+    partner = lax.rem(me + half, n)
+    plane = me // 2
+    at_end = (plane == 0) | (plane == n // 2 - 1)
+
+    def when_end(act):
+        if relayed:
+            pl.when(at_end)(act)
+
+    def when_middle(act):
+        if relayed:
+            pl.when(jnp.logical_not(at_end))(act)
+        else:
+            act()
+
+    def when_passing(act):
+        if relayed:
+            pl.when(jnp.logical_not(at_end))(act)
+
     first_row = pl.multiple_of(place * row_count, row_count)
     loads = [
         pltpu.make_async_copy(source, target, load_sem.at[i])
@@ -212,24 +251,46 @@
     after = lax.broadcasted_iota(jnp.int32, (row_count, row_count), 1)
     earlier = (before < after).astype(BF16)
     ranks = jnp.dot(hits.astype(BF16), earlier, preferred_element_type=F32)
-    ranks_ref[...] = jnp.where(hits > 0.0, ranks, -1.0)
-    shares_ref[...] = shares
+    meta_ref[0] = jnp.where(hits > 0.0, ranks, -1.0)
+    meta_ref[1] = shares
     slot = lax.broadcasted_iota(jnp.int32, (slot_count, row_count), 0).astype(F32)
-    picks, blends = [], []
-    for e in range(n):
-        match = slot == ranks_ref[e : e + 1]
-        picks.append(jnp.where(match, 1.0, 0.0))
-        blends.append(jnp.where(match, shares_ref[e : e + 1], 0.0))
-    chooser_ref[...] = jnp.concatenate(picks, axis=0).astype(BF16)
+
+    def selection(ref, first, count, weighted):
+        parts = []
+        for j in range(count):
+            match = slot == ref[0, pl.ds(first + j, 1)]
+            parts.append(jnp.where(match, ref[1, pl.ds(first + j, 1)] if weighted else 1.0, 0.0))
+        return jnp.concatenate(parts, axis=0)
+
+    def split(weights):
+        high = weights.astype(BF16)
+        return high, (weights - high.astype(F32)).astype(BF16)
 
     loads[0].wait()
     rows_wide = resid_ref[...].astype(F32)
     mean_square = jnp.mean(rows_wide * rows_wide, axis=-1, keepdims=True)
-    own_rows = (rows_wide * lax.rsqrt(mean_square + EPS) * gain_ref[...]).astype(BF16)
+    rows_ref[...] = (rows_wide * lax.rsqrt(mean_square + EPS) * gain_ref[...]).astype(BF16)
+
+    def rows_copy(i):
+        return pltpu.make_async_remote_copy(
+            src_ref=(rows_ref, meta_ref)[i],
+            dst_ref=(rows_in, meta_in)[i],
+            send_sem=rows_sem.at[0, i],
+            recv_sem=rows_sem.at[1, i],
+            device_id={"ep": partner},
+            device_id_type=MESH,
+        )
+
+    @when_end
+    def _():
+        rows_copy(1).start()
+        rows_copy(0).start()
+
+    chooser_ref[...] = selection(meta_ref, 0, n, False).astype(BF16)
     for g in range(slot_total // row_count):
         at = slice(g * row_count, (g + 1) * row_count)
         slots_ref[at] = jnp.dot(
-            chooser_ref[at], own_rows, preferred_element_type=F32
+            chooser_ref[at], rows_ref[...], preferred_element_type=F32
         ).astype(BF16)
 
     def block(ref, index):
@@ -262,15 +323,28 @@
 
         lax.fori_loop(1, n, one, 0)
 
-    each_peer(lambda peer: slot_copy(peer, me).start())
+    def each_near(act):
+        def one(step, carry):
+            act(base + lax.rem(me - base + step, half))
+            return carry
+
+        lax.fori_loop(1, half, one, 0)
+
+    def each_far(act):
+        def one(step, carry):
+            act(other + lax.rem(me - base + step, half))
+            return carry
+
+        lax.fori_loop(0, half, one, 0)
+
+    when_middle(lambda: each_far(lambda peer: slot_copy(peer, me).start()))
+    each_near(lambda peer: slot_copy(peer, me).start())
     for i in range(2 + pieces):
         weight_copy(i, 0).start()
     here = pl.ds(pl.multiple_of(me * slot_count, slot_count), slot_count)
     arrived_ref[here] = slots_ref[here]
-    blend = jnp.concatenate(blends, axis=0).T
-    blend_high = blend.astype(BF16)
-    blend_ref[0] = blend_high
-    blend_ref[1] = (blend - blend_high.astype(F32)).astype(BF16)
+    for h in range(2):
+        blend_ref[h, 0], blend_ref[h, 1] = split(selection(meta_ref, h * half, half, True).T)
 
     for load in loads[1:6]:
         load.wait()
@@ -349,7 +423,38 @@
         weight_copy(i, 0).wait_recv()
     weight_copy(0, 1).wait_recv()
     weight_copy(0, 2).start()
-    each_peer(lambda peer: slot_copy(peer, peer).wait_recv())
+
+    def pass_copy(target):
+        return pltpu.make_async_remote_copy(
+            src_ref=block(passed_ref, target - base),
+            dst_ref=block(arrived_ref, partner),
+            send_sem=pass_send.at[target - base],
+            recv_sem=slot_recv.at[partner],
+            device_id={"ep": target},
+            device_id_type=MESH,
+        )
+
+    @when_passing
+    def _():
+        rows_copy(1).wait_recv()
+        rows_copy(0).wait_recv()
+        chosen = selection(meta_in, base, half, False).astype(BF16)
+        passed_ref[...] = jnp.dot(chosen, rows_in[...], preferred_element_type=F32).astype(BF16)
+        each_near(lambda peer: pass_copy(peer).start())
+        arrived_ref[pl.ds(pl.multiple_of(partner * slot_count, slot_count), slot_count)] = (
+            passed_ref[pl.ds(pl.multiple_of((me - base) * slot_count, slot_count), slot_count)]
+        )
+        merge_blend[0], merge_blend[1] = split(selection(meta_in, base, half, True).T)
+
+    each_near(lambda peer: slot_copy(peer, peer).wait_recv())
+
+    def far_slots(peer):
+        if relayed:
+            pl.when(at_end | (peer != partner))(lambda: slot_copy(peer, peer).wait_recv())
+        else:
+            slot_copy(peer, peer).wait_recv()
+
+    each_far(far_slots)
     activate(3)
     activate(0)
     weight_copy(1, 1).wait_recv()
@@ -359,6 +464,54 @@
     weight_copy(1, 2).wait_recv()
     activate(2)
 
+    mine = pl.ds(pl.multiple_of((me - base) * slot_count, slot_count), slot_count)
+
+    def merge_copy(c, dest, source):
+        return pltpu.make_async_remote_copy(
+            src_ref=block(leaving_ref.at[c], dest),
+            dst_ref=block(merge_in.at[c], source - base),
+            send_sem=merge_send.at[c, dest],
+            recv_sem=merge_recv.at[c, source],
+            device_id={"ep": lax.rem(dest + half, n)},
+            device_id_type=MESH,
+        )
+
+    def far_back(c, peer, act):
+        if not relayed:
+            getattr(back_copy(c, peer, me), act)()
+            return
+        far_plane = peer // 2
+        far_end = (far_plane == 0) | (far_plane == n // 2 - 1)
+
+        @pl.when(far_end & (peer != partner))
+        def _():
+            getattr(merge_copy(c, peer, me), act)()
+
+        @pl.when(jnp.logical_not(far_end))
+        def _():
+            getattr(back_copy(c, peer, me), act)()
+
+    def merged_copy(c):
+        return pltpu.make_async_remote_copy(
+            src_ref=merged_ref.at[c],
+            dst_ref=merged_in.at[c],
+            send_sem=merged_send.at[c],
+            recv_sem=merged_recv.at[c],
+            device_id={"ep": partner},
+            device_id_type=MESH,
+        )
+
+    def blended(weights, values):
+        total = jnp.dot(weights[0], values, preferred_element_type=F32)
+        return total + jnp.dot(weights[1], values, preferred_element_type=F32)
+
+    def merge(c):
+        @when_passing
+        def _():
+            each_near(lambda peer: merge_copy(c, partner, peer).wait_recv())
+            merged_ref[c] = blended(merge_blend, merge_in[c]).astype(BF16)
+            merged_copy(c).start()
+
     def results(c):
         weight_copy(2 + c, 1).wait_recv()
         weight_copy(2 + c, 2).start()
@@ -366,15 +519,33 @@
         leaving_ref[c] = jnp.dot(
             active_ref[...], downs_ref[c], preferred_element_type=F32
         ).astype(BF16)
-        each_peer(lambda peer: back_copy(c, peer, me).start())
+        each_far(lambda peer: far_back(c, peer, "start"))
+        each_near(lambda peer: back_copy(c, peer, me).start())
         returned_ref[c, here] = leaving_ref[c, here]
 
+        @when_passing
+        def _():
+            merge_in[c, mine] = leaving_ref[
+                c, pl.ds(pl.multiple_of(partner * slot_count, slot_count), slot_count)
+            ]
+
     def collect(c):
-        each_peer(lambda peer: back_copy(c, peer, peer).wait_recv())
-        came = returned_ref[c]
-        total = jnp.dot(blend_ref[0], came, preferred_element_type=F32)
-        total = total + jnp.dot(blend_ref[1], came, preferred_element_type=F32)
-        routed_ref[:, c * span : (c + 1) * span] = total.astype(BF16)
+        each_near(lambda peer: back_copy(c, peer, peer).wait_recv())
+        near = returned_ref[c, pl.ds(pl.multiple_of(base * slot_count, side), side)]
+        total_ref[...] = blended(blend_ref.at[base // half], near)
+
+        @when_middle
+        def _():
+            each_far(lambda peer: back_copy(c, peer, peer).wait_recv())
+            far = returned_ref[c, pl.ds(pl.multiple_of(other * slot_count, side), side)]
+            total_ref[...] += blended(blend_ref.at[other // half], far)
+
+        @when_end
+        def _():
+            merged_copy(c).wait_recv()
+            total_ref[...] += merged_in[c].astype(F32)
+
+        routed_ref[:, c * span : (c + 1) * span] = total_ref[...].astype(BF16)
 
     def finish_mixer():
         each_peer(lambda peer: state_copy(peer, peer).wait_recv())
@@ -401,55 +572,78 @@
                 opened = combined * lax.rsqrt(mean_square + EPS) * scale_ref[:, lanes]
                 hidden_ref[at, lanes] = (opened * (gate / (1.0 + jnp.exp(-gate)))).astype(BF16)
 
-    def piece_copy(target, source):
+    diagonal = lax.rem(beside + quarters // 2, quarters)
+
+    def piece_copy(i):
         return pltpu.make_async_remote_copy(
-            src_ref=partial_ref.at[target],
-            dst_ref=pieces_ref.at[source],
-            send_sem=piece_send.at[target],
-            recv_sem=piece_recv.at[source],
-            device_id={"tp": target},
+            src_ref=(partial_ref.at[0], partial_ref.at[1], summed_ref)[i],
+            dst_ref=pieces_ref.at[i],
+            send_sem=piece_send.at[i],
+            recv_sem=piece_recv.at[i],
+            device_id={"tp": across if i == 2 else beside},
             device_id_type=MESH,
         )
 
-    def each_part(act):
-        def one(step, carry):
-            act(lax.rem(place + step, quarters))
-            return carry
-
-        lax.fori_loop(1, quarters, one, 0)
-
     def project():
-        for part in range(quarters):
-            at = slice(part * row_count, (part + 1) * row_count)
-            partial_ref[part] = jnp.dot(
+        for i, part in enumerate((diagonal, beside, across, place)):
+            at = pl.ds(pl.multiple_of(part * row_count, row_count), row_count)
+            partial_ref[i] = jnp.dot(
                 hidden_ref[at], proj_ref[...], preferred_element_type=F32
             ).astype(BF16)
-        each_part(lambda peer: piece_copy(peer, place).start())
-        pieces_ref[place] = partial_ref[place]
+            if i < 2:
+                piece_copy(i).start()
+
+    def cross():
+        piece_copy(0).wait_recv()
+        summed_ref[...] = (partial_ref[2].astype(F32) + pieces_ref[0].astype(F32)).astype(BF16)
+        piece_copy(2).start()
 
     def gather_mixed():
-        each_part(lambda peer: piece_copy(peer, peer).wait_recv())
-        total = pieces_ref[0].astype(F32)
-        for part in range(1, quarters):
-            total = total + pieces_ref[part].astype(F32)
-        mixed_ref[...] = total.astype(BF16)
+        piece_copy(1).wait_recv()
+        piece_copy(2).wait_recv()
+        total = partial_ref[3].astype(F32) + pieces_ref[1].astype(F32)
+        mixed_ref[...] = (total + pieces_ref[2].astype(F32)).astype(BF16)
 
     results(0)
+    results(1)
     finish_mixer()
-    results(1)
+    results(2)
     project()
-    for c in range(2, pieces):
+    merge(0)
+    results(3)
+    cross()
+    merge(1)
+    for c in range(4, pieces):
         results(c)
-    for c in range(pieces - 1):
+        merge(c - 2)
+    collect(0)
+    merge(pieces - 2)
+    collect(1)
+    merge(pieces - 1)
+    for c in range(2, pieces - 1):
         collect(c)
     gather_mixed()
     collect(pieces - 1)
 
-    each_peer(lambda peer: slot_copy(peer, peer).wait_send())
+    @when_end
+    def _():
+        rows_copy(0).wait_send()
+        rows_copy(1).wait_send()
+
+    when_middle(lambda: each_far(lambda peer: slot_copy(peer, me).wait_send()))
+    each_near(lambda peer: slot_copy(peer, me).wait_send())
+    when_passing(lambda: each_near(lambda peer: pass_copy(peer).wait_send()))
     each_peer(lambda peer: state_copy(peer, peer).wait_send())
-    for c in range(pieces):
-        each_peer(lambda peer, c=c: back_copy(c, peer, peer).wait_send())
-    each_part(lambda peer: piece_copy(peer, peer).wait_send())
+
+    def leave(c, carry):
+        each_far(lambda peer: far_back(c, peer, "wait_send"))
+        each_near(lambda peer: back_copy(c, peer, me).wait_send())
+        when_passing(lambda: merged_copy(c).wait_send())
+        return carry
+
+    lax.fori_loop(0, pieces, leave, 0)
+    for i in range(3):
+        piece_copy(i).wait_send()
     for i in range(2 + pieces):
         for hop in range(3):
             weight_copy(i, hop).wait_send()
@@ -506,18 +700,26 @@
         + [
             pltpu.VMEM((width, width_model), BF16),
             pltpu.VMEM((row_count, width_model), BF16),
-            pltpu.VMEM((n, row_count), F32),
-            pltpu.VMEM((n, row_count), F32),
+            pltpu.VMEM((2, n, row_count), F32),
+            pltpu.VMEM((2, n, row_count), F32),
+            pltpu.VMEM((row_count, width_model), BF16),
+            pltpu.VMEM((row_count, width_model), BF16),
             pltpu.VMEM((slot_total, row_count), BF16),
-            pltpu.VMEM((2, row_count, slot_total), BF16),
+            pltpu.VMEM((2, 2, row_count, slot_total // 2), BF16),
+            pltpu.VMEM((2, row_count, slot_total // 2), BF16),
             pltpu.VMEM((slot_total, width_model), BF16),
             pltpu.VMEM((slot_total, width_model), BF16),
+            pltpu.VMEM((slot_total // 2, width_model), BF16),
             pltpu.VMEM((quarters,) + expert_gate_matrix.shape[1:], BF16),
             pltpu.VMEM((quarters,) + expert_up_matrix.shape[1:], BF16),
             pltpu.VMEM((PIECES, quarters * units, span), BF16),
             pltpu.VMEM((slot_total, quarters * units), BF16),
             pltpu.VMEM((PIECES, slot_total, span), BF16),
             pltpu.VMEM((PIECES, slot_total, span), BF16),
+            pltpu.VMEM((PIECES, slot_total // 2, span), BF16),
+            pltpu.VMEM((PIECES, row_count, span), BF16),
+            pltpu.VMEM((PIECES, row_count, span), BF16),
+            pltpu.VMEM((row_count, span), F32),
             pltpu.VMEM((heads, chunks, CHUNK, depth), F32),
             pltpu.VMEM((2, heads, chunks, CHUNK, channels), BF16),
             pltpu.VMEM((2, heads, chunks, depth, channels), F32),
@@ -525,9 +727,16 @@
             pltpu.VMEM((2,) + state, BF16),
             pltpu.VMEM((n,) + state, BF16),
             pltpu.VMEM(block, BF16),
-            pltpu.VMEM((quarters, row_count, width_model), BF16),
-            pltpu.VMEM((quarters, row_count, width_model), BF16),
+            pltpu.VMEM((4, row_count, width_model), BF16),
+            pltpu.VMEM((row_count, width_model), BF16),
+            pltpu.VMEM((3, row_count, width_model), BF16),
             dma((9 + PIECES,)),
+            dma((2, 2)),
+            dma((n // 2,)),
+            dma((PIECES, n)),
+            dma((PIECES, n)),
+            dma((PIECES,)),
+            dma((PIECES,)),
             dma((n,)),
             dma((n,)),
             dma((n,)),
@@ -536,34 +745,39 @@
             dma((2 + PIECES, 3)),
             dma((PIECES, n)),
             dma((PIECES, n)),
-            dma((quarters,)),
-            dma((quarters,)),
+            dma((3,)),
+            dma((3,)),
         ],
         compiler_params=pltpu.CompilerParams(
-            collective_id=0, has_side_effects=True, vmem_limit_bytes=60 * 2**20
+            collective_id=0, has_side_effects=True, vmem_limit_bytes=48 * 2**20
         ),
         cost_estimate=pl.CostEstimate(
             flops=4 * 10**10, bytes_accessed=30 * 2**20, transcendentals=0
         ),
         name="mix_and_route",
     )(
-        queries,
-        forget_forward_logits,
-        forget_backward_logits,
-        values,
-        output_gate_logits,
-        lower_bound_forward.reshape(1, -1),
-        lower_bound_backward.reshape(1, -1),
-        extra_log_decay.T,
-        head_norm_scale.reshape(1, -1),
-        output_projection,
-        second_residual,
-        expert_norm_scale.reshape(1, -1),
-        routes.T,
-        specialist_mixing_factor.T,
-        expert_gate_matrix,
-        expert_up_matrix,
-        expert_down_matrix,
+        *(
+            pltpu.with_memory_space_constraint(operand, pltpu.HBM)
+            for operand in (
+                queries,
+                forget_forward_logits,
+                forget_backward_logits,
+                values,
+                output_gate_logits,
+                lower_bound_forward.reshape(1, -1),
+                lower_bound_backward.reshape(1, -1),
+                extra_log_decay.T,
+                head_norm_scale.reshape(1, -1),
+                output_projection,
+                second_residual,
+                expert_norm_scale.reshape(1, -1),
+                routes.T,
+                specialist_mixing_factor.T,
+                expert_gate_matrix,
+                expert_up_matrix,
+                expert_down_matrix,
+            )
+        )
     )
 
 

time: 117 us -> 105 us (0.90)
  Pallas kernels: 112 us -> 102 us
  local copies, waits for them, and re-layouts: 3.76 us -> 1.59 us
    pallas_call x1, Pallas kernels: 112 us -> 102 us  [shards(): pl.pallas_call(functools.partial(fused_kernel, n, quarters), out_shape=(o...]
    unnamed x2, local copies, waits for them, and re-layouts: 3.76 us -> 1.59 us
where the time goes in v2:
time: 105 us; the launch traced here: 104 us
  Pallas kernels  102 us (97%)
  local copies, waits for them, and re-layouts  1.59 us (2%)
    pallas_call x1, Pallas kernels, shards(): pl.pallas_call(functools.partial(fused_kernel, n, quarters), out_shape=(o...  102 us

profile of v2, /device:TPU:0, one launch (start us, length us, event | category | flops | bytes accessed | tf_op | source)
XLA Modules:
  0.0 104.1 jit_solution(3841536619899174470)
XLA Ops:
  0.6 101.8 %mix_and_route.1 = (bf16[128,2048]{1,0:T(8,128)(2,1)S(1)}, bf16[128,2048]{1,0:T(8,128)(2,1)S(1)}) custom-call(bf16[512,256]{1,0:T(8,128)(2,1)} %q_any.1, bf16[512,256]{1,0:T(8,128)(2,1)} %ff_any.1, bf16[512,256]{1,0:T(8,128)(2,1)} %fb_any.1, bf16[512,256]{1,0:T(8,128)(2,1)} %v_any.1, bf16[512,256]{1,0:T(8,128)(2,1)} %og_any.1, f32[1,256]{1,0:T(1,128)} %bitcast.10, ...), custom_call_target="tpu_custom_call" | custom-call | flops 40000000000 | bytes 31457280 | tf_op jit(solution)/shard_map/mix_and_route/pallas_call | solution.py:690
  102.5 0.8 copy.21
  103.3 0.8 copy.22

commit v3 on v2

--- a/solution.py
+++ b/solution.py
@@ -116,6 +116,7 @@
     gates_ref,
     ups_ref,
     downs_ref,
+    gated_ref,
     active_ref,
     leaving_ref,
     returned_ref,
@@ -136,7 +137,6 @@
     load_sem,
     rows_sem,
     pass_send,
-    merge_send,
     merge_recv,
     merged_send,
     merged_recv,
@@ -187,6 +187,8 @@
         if relayed:
             pl.when(jnp.logical_not(at_end))(act)
 
+    greet("ep", n)
+    greet("tp", quarters)
     first_row = pl.multiple_of(place * row_count, row_count)
     loads = [
         pltpu.make_async_copy(source, target, load_sem.at[i])
@@ -202,20 +204,19 @@
                 (gate_any.at[0], gates_ref.at[3]),
                 (up_any.at[0], ups_ref.at[3]),
             )
-            + tuple(
-                (
-                    down_any.at[0, :, c * span : (c + 1) * span],
-                    downs_ref.at[c, 3 * units : 4 * units],
-                )
-                for c in range(pieces)
-            )
         )
     ]
-    for load in loads:
+    down_loads = [
+        pltpu.make_async_copy(
+            down_any.at[0, :, c * span : (c + 1) * span],
+            downs_ref.at[c, 3 * units : 4 * units],
+            load_sem.at[9],
+        )
+        for c in range(pieces)
+    ]
+    for load in loads + down_loads:
         load.start()
 
-    greet("ep", n)
-    greet("tp", quarters)
     pl.semaphore_wait(pltpu.get_barrier_semaphore(), n + quarters - 2)
 
     def weight_copy(i, hop):
@@ -230,8 +231,8 @@
         return pltpu.make_async_remote_copy(
             src_ref=passed if hop == 2 else own,
             dst_ref=target,
-            send_sem=weight_send.at[i, hop],
-            recv_sem=weight_recv.at[i, hop],
+            send_sem=weight_send.at[min(i, 2), hop],
+            recv_sem=weight_recv.at[min(i, 2) if hop == 0 else i, hop],
             device_id={"tp": across if hop == 1 else beside},
             device_id_type=MESH,
         )
@@ -296,22 +297,32 @@
     def block(ref, index):
         return ref.at[pl.ds(pl.multiple_of(index * slot_count, slot_count), slot_count)]
 
-    def slot_copy(target, source):
+    def slot_copy(target, far):
         return pltpu.make_async_remote_copy(
             src_ref=block(slots_ref, target),
-            dst_ref=block(arrived_ref, source),
-            send_sem=slot_send.at[target],
-            recv_sem=slot_recv.at[source],
+            dst_ref=block(arrived_ref, me),
+            send_sem=slot_send,
+            recv_sem=slot_recv.at[far],
             device_id={"ep": target},
             device_id_type=MESH,
         )
 
-    def back_copy(c, target, source):
+    def settle(ref, semaphore):
+        return pltpu.make_async_remote_copy(
+            src_ref=ref,
+            dst_ref=ref,
+            send_sem=semaphore,
+            recv_sem=semaphore,
+            device_id={"ep": partner},
+            device_id_type=MESH,
+        )
+
+    def back_copy(c, target, far):
         return pltpu.make_async_remote_copy(
             src_ref=block(leaving_ref.at[c], target),
-            dst_ref=block(returned_ref.at[c], source),
-            send_sem=back_send.at[c, target],
-            recv_sem=back_recv.at[c, source],
+            dst_ref=block(returned_ref.at[c], me),
+            send_sem=back_send,
+            recv_sem=back_recv.at[c, far],
             device_id={"ep": target},
             device_id_type=MESH,
         )
@@ -337,8 +348,8 @@
 
         lax.fori_loop(0, half, one, 0)
 
-    when_middle(lambda: each_far(lambda peer: slot_copy(peer, me).start()))
-    each_near(lambda peer: slot_copy(peer, me).start())
+    when_middle(lambda: each_far(lambda peer: slot_copy(peer, 1).start()))
+    each_near(lambda peer: slot_copy(peer, 0).start())
     for i in range(2 + pieces):
         weight_copy(i, 0).start()
     here = pl.ds(pl.multiple_of(me * slot_count, slot_count), slot_count)
@@ -396,40 +407,25 @@
                 fade, (DECAY_ROWS, channels)
             ).astype(BF16)
 
-    def state_copy(target, source):
+    def state_copy(target):
         way = jnp.where(target > me, 0, 1)
         return pltpu.make_async_remote_copy(
             src_ref=state_out.at[way],
-            dst_ref=state_in.at[source],
-            send_sem=state_send.at[target],
-            recv_sem=state_recv.at[source],
+            dst_ref=state_in.at[me],
+            send_sem=state_send,
+            recv_sem=state_recv,
             device_id={"ep": target},
             device_id_type=MESH,
         )
 
-    each_peer(lambda peer: state_copy(peer, me).start())
-
-    def activate(i):
-        arrived = arrived_ref[...]
-        gated = jnp.dot(arrived, gates_ref[i], preferred_element_type=F32)
-        lifted = jnp.dot(arrived, ups_ref[i], preferred_element_type=F32)
-        active_ref[:, i * units : (i + 1) * units] = (
-            gated / (1.0 + jnp.exp(-gated)) * lifted
-        ).astype(BF16)
-
-    for load in loads[6:]:
-        load.wait()
-    for i in range(2 + pieces):
-        weight_copy(i, 0).wait_recv()
-    weight_copy(0, 1).wait_recv()
-    weight_copy(0, 2).start()
+    each_peer(lambda peer: state_copy(peer).start())
 
     def pass_copy(target):
         return pltpu.make_async_remote_copy(
             src_ref=block(passed_ref, target - base),
             dst_ref=block(arrived_ref, partner),
-            send_sem=pass_send.at[target - base],
-            recv_sem=slot_recv.at[partner],
+            send_sem=pass_send,
+            recv_sem=slot_recv.at[1],
             device_id={"ep": target},
             device_id_type=MESH,
         )
@@ -446,56 +442,74 @@
         )
         merge_blend[0], merge_blend[1] = split(selection(meta_in, base, half, True).T)
 
-    each_near(lambda peer: slot_copy(peer, peer).wait_recv())
-
-    def far_slots(peer):
-        if relayed:
-            pl.when(at_end | (peer != partner))(lambda: slot_copy(peer, peer).wait_recv())
-        else:
-            slot_copy(peer, peer).wait_recv()
-
-    each_far(far_slots)
-    activate(3)
-    activate(0)
+    near_rows = pl.ds(pl.multiple_of(base * slot_count, side), side)
+    far_rows = pl.ds(pl.multiple_of(other * slot_count, side), side)
+
+    def open_gate(i, at):
+        gated = jnp.dot(arrived_ref[at], gates_ref[i], preferred_element_type=F32)
+        gated_ref[at, i * units : (i + 1) * units] = gated / (1.0 + jnp.exp(-gated))
+
+    def activate(i, at):
+        lifted = jnp.dot(arrived_ref[at], ups_ref[i], preferred_element_type=F32)
+        columns = slice(i * units, (i + 1) * units)
+        active_ref[at, columns] = (gated_ref[at, columns] * lifted).astype(BF16)
+
+    for load in loads[6:]:
+        load.wait()
+    settle(downs_ref.at[:, 3 * units : 4 * units], load_sem.at[9]).wait_recv()
+    weight_copy(0, 0).wait_recv()
+    weight_copy(1, 0).wait_recv()
+    settle(downs_ref.at[:, :units], weight_recv.at[2, 0]).wait_recv()
+    settle(arrived_ref.at[: (half - 1) * slot_count], slot_recv.at[0]).wait_recv()
+    for i in (3, 0):
+        open_gate(i, near_rows)
+        activate(i, near_rows)
+    weight_copy(0, 1).wait_recv()
+    weight_copy(0, 2).start()
+    open_gate(1, near_rows)
+    weight_copy(0, 2).wait_recv()
+    open_gate(2, near_rows)
+
+    @when_end
+    def _():
+        settle(arrived_ref.at[: half * slot_count], slot_recv.at[1]).wait_recv()
+
+    @when_middle
+    def _():
+        blocks = half - 1 if relayed else half
+        settle(arrived_ref.at[: blocks * slot_count], slot_recv.at[1]).wait_recv()
+
+    for i in (3, 0):
+        open_gate(i, far_rows)
+        activate(i, far_rows)
+    open_gate(1, far_rows)
+    open_gate(2, far_rows)
     weight_copy(1, 1).wait_recv()
     weight_copy(1, 2).start()
-    activate(1)
-    weight_copy(0, 2).wait_recv()
+    activate(1, slice(None))
     weight_copy(1, 2).wait_recv()
-    activate(2)
+    activate(2, slice(None))
 
     mine = pl.ds(pl.multiple_of((me - base) * slot_count, slot_count), slot_count)
 
-    def merge_copy(c, dest, source):
+    def merge_copy(c, dest):
         return pltpu.make_async_remote_copy(
             src_ref=block(leaving_ref.at[c], dest),
-            dst_ref=block(merge_in.at[c], source - base),
-            send_sem=merge_send.at[c, dest],
-            recv_sem=merge_recv.at[c, source],
+            dst_ref=block(merge_in.at[c], me - base),
+            send_sem=back_send,
+            recv_sem=merge_recv.at[c],
             device_id={"ep": lax.rem(dest + half, n)},
             device_id_type=MESH,
         )
 
-    def far_back(c, peer, act):
-        if not relayed:
-            getattr(back_copy(c, peer, me), act)()
-            return
-        far_plane = peer // 2
-        far_end = (far_plane == 0) | (far_plane == n // 2 - 1)
-
-        @pl.when(far_end & (peer != partner))
-        def _():
-            getattr(merge_copy(c, peer, me), act)()
-
-        @pl.when(jnp.logical_not(far_end))
-        def _():
-            getattr(back_copy(c, peer, me), act)()
+    def ends(peer):
+        return (peer // 2 == 0) | (peer // 2 == n // 2 - 1)
 
     def merged_copy(c):
         return pltpu.make_async_remote_copy(
             src_ref=merged_ref.at[c],
             dst_ref=merged_in.at[c],
-            send_sem=merged_send.at[c],
+            send_sem=merged_send,
             recv_sem=merged_recv.at[c],
             device_id={"ep": partner},
             device_id_type=MESH,
@@ -508,7 +522,7 @@
     def merge(c):
         @when_passing
         def _():
-            each_near(lambda peer: merge_copy(c, partner, peer).wait_recv())
+            settle(merge_in.at[c, : (half - 1) * slot_count], merge_recv.at[c]).wait_recv()
             merged_ref[c] = blended(merge_blend, merge_in[c]).astype(BF16)
             merged_copy(c).start()
 
@@ -519,9 +533,6 @@
         leaving_ref[c] = jnp.dot(
             active_ref[...], downs_ref[c], preferred_element_type=F32
         ).astype(BF16)
-        each_far(lambda peer: far_back(c, peer, "start"))
-        each_near(lambda peer: back_copy(c, peer, me).start())
-        returned_ref[c, here] = leaving_ref[c, here]
 
         @when_passing
         def _():
@@ -529,16 +540,31 @@
                 c, pl.ds(pl.multiple_of(partner * slot_count, slot_count), slot_count)
             ]
 
+        if relayed:
+
+            @each_far
+            def _(peer):
+                pl.when(ends(peer) & (peer != partner))(lambda: merge_copy(c, peer).start())
+
+    def direct(c):
+        @each_far
+        def _(peer):
+            if relayed:
+                pl.when(jnp.logical_not(ends(peer)))(lambda: back_copy(c, peer, 1).start())
+            else:
+                back_copy(c, peer, 1).start()
+
+        each_near(lambda peer: back_copy(c, peer, 0).start())
+        returned_ref[c, here] = leaving_ref[c, here]
+
     def collect(c):
-        each_near(lambda peer: back_copy(c, peer, peer).wait_recv())
-        near = returned_ref[c, pl.ds(pl.multiple_of(base * slot_count, side), side)]
-        total_ref[...] = blended(blend_ref.at[base // half], near)
+        settle(returned_ref.at[c, : (half - 1) * slot_count], back_recv.at[c, 0]).wait_recv()
+        total_ref[...] = blended(blend_ref.at[base // half], returned_ref[c, near_rows])
 
         @when_middle
         def _():
-            each_far(lambda peer: back_copy(c, peer, peer).wait_recv())
-            far = returned_ref[c, pl.ds(pl.multiple_of(other * slot_count, side), side)]
-            total_ref[...] += blended(blend_ref.at[other // half], far)
+            settle(returned_ref.at[c, : half * slot_count], back_recv.at[c, 1]).wait_recv()
+            total_ref[...] += blended(blend_ref.at[other // half], returned_ref[c, far_rows])
 
         @when_end
         def _():
@@ -548,7 +574,7 @@
         routed_ref[:, c * span : (c + 1) * span] = total_ref[...].astype(BF16)
 
     def finish_mixer():
-        each_peer(lambda peer: state_copy(peer, peer).wait_recv())
+        settle(state_in.at[: n - 1], state_recv).wait_recv()
         depth = part_ref.shape[3]
         for h in range(heads):
             for way in range(2):
@@ -605,22 +631,24 @@
         mixed_ref[...] = (total + pieces_ref[2].astype(F32)).astype(BF16)
 
     results(0)
+    direct(0)
     results(1)
     finish_mixer()
-    results(2)
-    project()
-    merge(0)
-    results(3)
-    cross()
-    merge(1)
-    for c in range(4, pieces):
+    for c in range(2, pieces):
         results(c)
         merge(c - 2)
+        direct(c - 1)
+        if c == 2:
+            project()
+        if c == 3:
+            cross()
     collect(0)
+    collect(1)
     merge(pieces - 2)
-    collect(1)
+    collect(2)
     merge(pieces - 1)
-    for c in range(2, pieces - 1):
+    direct(pieces - 1)
+    for c in range(3, pieces - 1):
         collect(c)
     gather_mixed()
     collect(pieces - 1)
@@ -629,24 +657,27 @@
     def _():
         rows_copy(0).wait_send()
         rows_copy(1).wait_send()
-
-    when_middle(lambda: each_far(lambda peer: slot_copy(peer, me).wait_send()))
-    each_near(lambda peer: slot_copy(peer, me).wait_send())
-    when_passing(lambda: each_near(lambda peer: pass_copy(peer).wait_send()))
-    each_peer(lambda peer: state_copy(peer, peer).wait_send())
-
-    def leave(c, carry):
-        each_far(lambda peer: far_back(c, peer, "wait_send"))
-        each_near(lambda peer: back_copy(c, peer, me).wait_send())
-        when_passing(lambda: merged_copy(c).wait_send())
-        return carry
-
-    lax.fori_loop(0, pieces, leave, 0)
+        settle(slots_ref.at[: (half - 1) * slot_count], slot_send).wait_send()
+        settle(leaving_ref.at[:, : (n - 1) * slot_count], back_send).wait_send()
+
+    @when_middle
+    def _():
+        blocks = n - 2 if relayed else n - 1
+        settle(slots_ref.at[: (n - 1) * slot_count], slot_send).wait_send()
+        settle(leaving_ref.at[:, : blocks * slot_count], back_send).wait_send()
+
+    @when_passing
+    def _():
+        settle(passed_ref.at[: (half - 1) * slot_count], pass_send).wait_send()
+        settle(merged_ref, merged_send).wait_send()
+
+    settle(state_in.at[: n - 1], state_send).wait_send()
     for i in range(3):
         piece_copy(i).wait_send()
-    for i in range(2 + pieces):
-        for hop in range(3):
-            weight_copy(i, hop).wait_send()
+    for hop in range(3):
+        settle(gates_ref.at[0], weight_send.at[0, hop]).wait_send()
+        settle(ups_ref.at[0], weight_send.at[1, hop]).wait_send()
+        settle(downs_ref.at[:, :units], weight_send.at[2, hop]).wait_send()
 
 
 def shards(
@@ -713,6 +744,7 @@
             pltpu.VMEM((quarters,) + expert_gate_matrix.shape[1:], BF16),
             pltpu.VMEM((quarters,) + expert_up_matrix.shape[1:], BF16),
             pltpu.VMEM((PIECES, quarters * units, span), BF16),
+            pltpu.VMEM((slot_total, quarters * units), F32),
             pltpu.VMEM((slot_total, quarters * units), BF16),
             pltpu.VMEM((PIECES, slot_total, span), BF16),
             pltpu.VMEM((PIECES, slot_total, span), BF16),
@@ -730,21 +762,20 @@
             pltpu.VMEM((4, row_count, width_model), BF16),
             pltpu.VMEM((row_count, width_model), BF16),
             pltpu.VMEM((3, row_count, width_model), BF16),
-            dma((9 + PIECES,)),
+            dma((10,)),
             dma((2, 2)),
-            dma((n // 2,)),
-            dma((PIECES, n)),
-            dma((PIECES, n)),
+            dma(()),
             dma((PIECES,)),
+            dma(()),
             dma((PIECES,)),
-            dma((n,)),
-            dma((n,)),
-            dma((n,)),
-            dma((n,)),
+            dma(()),
+            dma((2,)),
+            dma(()),
+            dma(()),
+            dma((3, 3)),
             dma((2 + PIECES, 3)),
-            dma((2 + PIECES, 3)),
-            dma((PIECES, n)),
-            dma((PIECES, n)),
+            dma(()),
+            dma((PIECES, 2)),
             dma((3,)),
             dma((3,)),
         ],

time: 105 us -> 101 us (0.962)
  Pallas kernels: 102 us -> 98.1 us
    pallas_call x1, Pallas kernels: 102 us -> 98.1 us  [shards(): pl.pallas_call(functools.partial(fused_kernel, n, quarters), out_shape=(o...]
where the time goes in v3:
time: 101 us; the launch traced here: 100 us
  Pallas kernels  98.1 us (97%)
  local copies, waits for them, and re-layouts  1.59 us (2%)
    pallas_call x1, Pallas kernels, shards(): pl.pallas_call(functools.partial(fused_kernel, n, quarters), out_shape=(o...  98.1 us

profile of v3, /device:TPU:0, one launch (start us, length us, event | category | flops | bytes accessed | tf_op | source)
XLA Modules:
  0.0 100.4 jit_solution(2181432550215271590)
XLA Ops:
  0.6 98.1 %mix_and_route.1 = (bf16[128,2048]{1,0:T(8,128)(2,1)S(1)}, bf16[128,2048]{1,0:T(8,128)(2,1)S(1)}) custom-call(bf16[512,256]{1,0:T(8,128)(2,1)} %q_any.1, bf16[512,256]{1,0:T(8,128)(2,1)} %ff_any.1, bf16[512,256]{1,0:T(8,128)(2,1)} %fb_any.1, bf16[512,256]{1,0:T(8,128)(2,1)} %v_any.1, bf16[512,256]{1,0:T(8,128)(2,1)} %og_any.1, f32[1,256]{1,0:T(1,128)} %bitcast.10, ...), custom_call_target="tpu_custom_call" | custom-call | flops 40000000000 | bytes 31457280 | tf_op jit(solution)/shard_map/mix_and_route/pallas_call | solution.py:721
  98.8 0.8 copy.21
  99.6 0.8 copy.22

commit v4 on v3

--- a/solution.py
+++ b/solution.py
@@ -11,7 +11,8 @@
 CHUNK = 128
 LEAF = 16
 DECAY_ROWS = 16
-PIECES = 8
+SPANS = 16
+PIECES = SPANS // 2 + 1
 PLANES = 4
 EPS = 1e-06
 MESH = pl.DeviceIdType.MESH
@@ -115,14 +116,21 @@
     passed_ref,
     gates_ref,
     ups_ref,
-    downs_ref,
+    downs_ref_narrow,
+    downs_ref_wide,
     gated_ref,
     active_ref,
-    leaving_ref,
-    returned_ref,
-    merge_in,
-    merged_ref,
-    merged_in,
+    lifted_ref,
+    leaving_ref_narrow,
+    leaving_ref_wide,
+    returned_ref_narrow,
+    returned_ref_wide,
+    merge_in_narrow,
+    merge_in_wide,
+    merged_ref_narrow,
+    merged_ref_wide,
+    merged_in_narrow,
+    merged_in_wide,
     total_ref,
     local_ref,
     reach_ref,
@@ -146,7 +154,8 @@
     state_recv,
     weight_send,
     weight_recv,
-    back_send,
+    far_send,
+    near_send,
     back_recv,
     piece_send,
     piece_recv,
@@ -160,8 +169,31 @@
     channels = width // heads
     slot_total = slots_ref.shape[0]
     slot_count = slot_total // n
-    pieces, _, span = leaving_ref.shape
     units = down_any.shape[1]
+    depth_half = width_model // 2
+
+    pieces, span = PIECES, width_model // SPANS
+
+    def piece(refs, c):
+        narrow, wide = refs
+        return narrow.at[c // (pieces - 1)] if is_narrow(c) else wide.at[c - 1]
+
+    def is_narrow(c):
+        return c in (0, pieces - 1)
+
+    def far_group(c):
+        return 1 if is_narrow(c) else 2 if c == pieces - 2 else 0
+
+    def columns(c):
+        first = max(0, (2 * c - 1) * span)
+        return slice(first, first + (span if is_narrow(c) else 2 * span))
+
+    downs_refs = downs_ref_narrow, downs_ref_wide
+    leaving_refs = leaving_ref_narrow, leaving_ref_wide
+    returned_refs = returned_ref_narrow, returned_ref_wide
+    merge_refs = merge_in_narrow, merge_in_wide
+    merged_refs = merged_ref_narrow, merged_ref_wide
+    merged_in_refs = merged_in_narrow, merged_in_wide
     beside, across = neighbours()
 
     half = n // 2
@@ -194,6 +226,8 @@
         pltpu.make_async_copy(source, target, load_sem.at[i])
         for i, (source, target) in enumerate(
             (
+                (gate_any.at[0], gates_ref.at[3]),
+                (up_any.at[0], ups_ref.at[3]),
                 (resid_any.at[pl.ds(first_row, row_count)], resid_ref),
                 (q_any, q_ref),
                 (ff_any, ff_ref),
@@ -201,44 +235,51 @@
                 (v_any, v_ref),
                 (og_any, og_ref),
                 (proj_any, proj_ref),
-                (gate_any.at[0], gates_ref.at[3]),
-                (up_any.at[0], ups_ref.at[3]),
             )
         )
     ]
     down_loads = [
         pltpu.make_async_copy(
-            down_any.at[0, :, c * span : (c + 1) * span],
-            downs_ref.at[c, 3 * units : 4 * units],
-            load_sem.at[9],
+            down_any.at[0, :, columns(c)],
+            piece(downs_refs, c).at[3 * units : 4 * units],
+            load_sem.at[9 if is_narrow(c) else 10],
         )
         for c in range(pieces)
     ]
-    for load in loads + down_loads:
+    for load in loads[:2] + down_loads + loads[2:]:
         load.start()
 
     pl.semaphore_wait(pltpu.get_barrier_semaphore(), n + quarters - 2)
 
     def weight_copy(i, hop):
-        if i < 2:
-            own, held = ((gate_any.at[0], gates_ref), (up_any.at[0], ups_ref))[i]
-            target, passed = held.at[hop], held.at[1]
+        kind = min(i, 1)
+        if i == 0:
+            held = lambda slot: gates_ref.at[slot]
+        elif i < 3:
+            at = slice((i - 1) * depth_half, i * depth_half)
+            held = lambda slot: ups_ref.at[slot, at]
         else:
-            c = i - 2
-            own = down_any.at[0, :, c * span : (c + 1) * span]
-            target = downs_ref.at[c, hop * units : (hop + 1) * units]
-            passed = downs_ref.at[c, units : 2 * units]
+            kind = 2 if is_narrow(i - 3) else 3
+            held = lambda slot: piece(downs_refs, i - 3).at[slot * units : (slot + 1) * units]
         return pltpu.make_async_remote_copy(
-            src_ref=passed if hop == 2 else own,
-            dst_ref=target,
-            send_sem=weight_send.at[min(i, 2), hop],
-            recv_sem=weight_recv.at[min(i, 2) if hop == 0 else i, hop],
+            src_ref=held(1 if hop == 2 else 3),
+            dst_ref=held(hop),
+            send_sem=weight_send.at[kind, hop],
+            recv_sem=weight_recv.at[kind if hop == 0 else i, hop],
             device_id={"tp": across if hop == 1 else beside},
             device_id_type=MESH,
         )
 
-    for i in range(2 + pieces):
+    loads[0].wait()
+    weight_copy(0, 1).start()
+    loads[1].wait()
+    for i in (1, 2):
         weight_copy(i, 1).start()
+    for kind in range(2):
+        own_part = downs_refs[kind].at[:, 3 * units : 4 * units]
+        pltpu.make_async_copy(own_part, own_part, load_sem.at[9 + kind]).wait()
+    for c in range(pieces):
+        weight_copy(3 + c, 1).start()
 
     lanes = pl.ds(first_row, row_count)
     expert = lax.broadcasted_iota(jnp.int32, (n, row_count), 0)
@@ -267,7 +308,7 @@
         high = weights.astype(BF16)
         return high, (weights - high.astype(F32)).astype(BF16)
 
-    loads[0].wait()
+    loads[2].wait()
     rows_wide = resid_ref[...].astype(F32)
     mean_square = jnp.mean(rows_wide * rows_wide, axis=-1, keepdims=True)
     rows_ref[...] = (rows_wide * lax.rsqrt(mean_square + EPS) * gain_ref[...]).astype(BF16)
@@ -319,9 +360,9 @@
 
     def back_copy(c, target, far):
         return pltpu.make_async_remote_copy(
-            src_ref=block(leaving_ref.at[c], target),
-            dst_ref=block(returned_ref.at[c], me),
-            send_sem=back_send,
+            src_ref=block(piece(leaving_refs, c), target),
+            dst_ref=block(piece(returned_refs, c), me),
+            send_sem=far_send.at[far_group(c)] if far else near_send.at[int(is_narrow(c))],
             recv_sem=back_recv.at[c, far],
             device_id={"ep": target},
             device_id_type=MESH,
@@ -350,14 +391,14 @@
 
     when_middle(lambda: each_far(lambda peer: slot_copy(peer, 1).start()))
     each_near(lambda peer: slot_copy(peer, 0).start())
-    for i in range(2 + pieces):
+    for i in range(3 + pieces):
         weight_copy(i, 0).start()
     here = pl.ds(pl.multiple_of(me * slot_count, slot_count), slot_count)
     arrived_ref[here] = slots_ref[here]
     for h in range(2):
         blend_ref[h, 0], blend_ref[h, 1] = split(selection(meta_ref, h * half, half, True).T)
 
-    for load in loads[1:6]:
+    for load in loads[3:]:
         load.wait()
     rows = lax.broadcasted_iota(jnp.int32, (CHUNK, CHUNK), 0)
     cols = lax.broadcasted_iota(jnp.int32, (CHUNK, CHUNK), 1)
@@ -449,129 +490,16 @@
         gated = jnp.dot(arrived_ref[at], gates_ref[i], preferred_element_type=F32)
         gated_ref[at, i * units : (i + 1) * units] = gated / (1.0 + jnp.exp(-gated))
 
-    def activate(i, at):
-        lifted = jnp.dot(arrived_ref[at], ups_ref[i], preferred_element_type=F32)
-        columns = slice(i * units, (i + 1) * units)
-        active_ref[at, columns] = (gated_ref[at, columns] * lifted).astype(BF16)
-
-    for load in loads[6:]:
-        load.wait()
-    settle(downs_ref.at[:, 3 * units : 4 * units], load_sem.at[9]).wait_recv()
-    weight_copy(0, 0).wait_recv()
-    weight_copy(1, 0).wait_recv()
-    settle(downs_ref.at[:, :units], weight_recv.at[2, 0]).wait_recv()
-    settle(arrived_ref.at[: (half - 1) * slot_count], slot_recv.at[0]).wait_recv()
-    for i in (3, 0):
-        open_gate(i, near_rows)
-        activate(i, near_rows)
-    weight_copy(0, 1).wait_recv()
-    weight_copy(0, 2).start()
-    open_gate(1, near_rows)
-    weight_copy(0, 2).wait_recv()
-    open_gate(2, near_rows)
-
-    @when_end
-    def _():
-        settle(arrived_ref.at[: half * slot_count], slot_recv.at[1]).wait_recv()
-
-    @when_middle
-    def _():
-        blocks = half - 1 if relayed else half
-        settle(arrived_ref.at[: blocks * slot_count], slot_recv.at[1]).wait_recv()
-
-    for i in (3, 0):
-        open_gate(i, far_rows)
-        activate(i, far_rows)
-    open_gate(1, far_rows)
-    open_gate(2, far_rows)
-    weight_copy(1, 1).wait_recv()
-    weight_copy(1, 2).start()
-    activate(1, slice(None))
-    weight_copy(1, 2).wait_recv()
-    activate(2, slice(None))
-
-    mine = pl.ds(pl.multiple_of((me - base) * slot_count, slot_count), slot_count)
-
-    def merge_copy(c, dest):
-        return pltpu.make_async_remote_copy(
-            src_ref=block(leaving_ref.at[c], dest),
-            dst_ref=block(merge_in.at[c], me - base),
-            send_sem=back_send,
-            recv_sem=merge_recv.at[c],
-            device_id={"ep": lax.rem(dest + half, n)},
-            device_id_type=MESH,
-        )
-
-    def ends(peer):
-        return (peer // 2 == 0) | (peer // 2 == n // 2 - 1)
-
-    def merged_copy(c):
-        return pltpu.make_async_remote_copy(
-            src_ref=merged_ref.at[c],
-            dst_ref=merged_in.at[c],
-            send_sem=merged_send,
-            recv_sem=merged_recv.at[c],
-            device_id={"ep": partner},
-            device_id_type=MESH,
-        )
-
-    def blended(weights, values):
-        total = jnp.dot(weights[0], values, preferred_element_type=F32)
-        return total + jnp.dot(weights[1], values, preferred_element_type=F32)
-
-    def merge(c):
-        @when_passing
-        def _():
-            settle(merge_in.at[c, : (half - 1) * slot_count], merge_recv.at[c]).wait_recv()
-            merged_ref[c] = blended(merge_blend, merge_in[c]).astype(BF16)
-            merged_copy(c).start()
-
-    def results(c):
-        weight_copy(2 + c, 1).wait_recv()
-        weight_copy(2 + c, 2).start()
-        weight_copy(2 + c, 2).wait_recv()
-        leaving_ref[c] = jnp.dot(
-            active_ref[...], downs_ref[c], preferred_element_type=F32
-        ).astype(BF16)
-
-        @when_passing
-        def _():
-            merge_in[c, mine] = leaving_ref[
-                c, pl.ds(pl.multiple_of(partner * slot_count, slot_count), slot_count)
-            ]
-
-        if relayed:
-
-            @each_far
-            def _(peer):
-                pl.when(ends(peer) & (peer != partner))(lambda: merge_copy(c, peer).start())
-
-    def direct(c):
-        @each_far
-        def _(peer):
-            if relayed:
-                pl.when(jnp.logical_not(ends(peer)))(lambda: back_copy(c, peer, 1).start())
-            else:
-                back_copy(c, peer, 1).start()
-
-        each_near(lambda peer: back_copy(c, peer, 0).start())
-        returned_ref[c, here] = leaving_ref[c, here]
-
-    def collect(c):
-        settle(returned_ref.at[c, : (half - 1) * slot_count], back_recv.at[c, 0]).wait_recv()
-        total_ref[...] = blended(blend_ref.at[base // half], returned_ref[c, near_rows])
-
-        @when_middle
-        def _():
-            settle(returned_ref.at[c, : half * slot_count], back_recv.at[c, 1]).wait_recv()
-            total_ref[...] += blended(blend_ref.at[other // half], returned_ref[c, far_rows])
-
-        @when_end
-        def _():
-            merged_copy(c).wait_recv()
-            total_ref[...] += merged_in[c].astype(F32)
-
-        routed_ref[:, c * span : (c + 1) * span] = total_ref[...].astype(BF16)
+    def lift(i, part, at):
+        rows_of = slice(part * depth_half, (part + 1) * depth_half)
+        return jnp.dot(arrived_ref[at, rows_of], ups_ref[i, rows_of], preferred_element_type=F32)
+
+    def activate(i, at, lifted):
+        hidden = slice(i * units, (i + 1) * units)
+        active_ref[at, hidden] = (gated_ref[at, hidden] * lifted).astype(BF16)
+
+    def activate_whole(i, at):
+        activate(i, at, jnp.dot(arrived_ref[at], ups_ref[i], preferred_element_type=F32))
 
     def finish_mixer():
         settle(state_in.at[: n - 1], state_recv).wait_recv()
@@ -598,6 +526,136 @@
                 opened = combined * lax.rsqrt(mean_square + EPS) * scale_ref[:, lanes]
                 hidden_ref[at, lanes] = (opened * (gate / (1.0 + jnp.exp(-gate)))).astype(BF16)
 
+    every = slice(None)
+    for kind in range(2):
+        settle(downs_refs[kind].at[:, :units], weight_recv.at[2 + kind, 0]).wait_recv()
+    weight_copy(0, 0).wait_recv()
+    settle(ups_ref.at[0], weight_recv.at[1, 0]).wait_recv()
+    settle(arrived_ref.at[: (half - 1) * slot_count], slot_recv.at[0]).wait_recv()
+    for i in (3, 0):
+        open_gate(i, near_rows)
+        activate_whole(i, near_rows)
+    weight_copy(0, 1).wait_recv()
+    weight_copy(0, 2).start()
+    open_gate(1, near_rows)
+    weight_copy(0, 2).wait_recv()
+    open_gate(2, near_rows)
+    weight_copy(1, 1).wait_recv()
+    weight_copy(1, 2).start()
+
+    @when_end
+    def _():
+        settle(arrived_ref.at[: half * slot_count], slot_recv.at[1]).wait_recv()
+
+    @when_middle
+    def _():
+        blocks = half - 1 if relayed else half
+        settle(arrived_ref.at[: blocks * slot_count], slot_recv.at[1]).wait_recv()
+
+    for i in (3, 0):
+        open_gate(i, far_rows)
+        activate_whole(i, far_rows)
+    open_gate(1, far_rows)
+    open_gate(2, far_rows)
+    lifted_ref[0] = lift(1, 0, every)
+    weight_copy(1, 2).wait_recv()
+    lifted_ref[1] = lift(2, 0, every)
+    weight_copy(2, 1).wait_recv()
+    weight_copy(2, 2).start()
+    activate(1, every, lifted_ref[0] + lift(1, 1, every))
+    weight_copy(3, 1).wait_recv()
+    weight_copy(3, 2).start()
+    weight_copy(2, 2).wait_recv()
+    activate(2, every, lifted_ref[1] + lift(2, 1, every))
+
+    mine = pl.ds(pl.multiple_of((me - base) * slot_count, slot_count), slot_count)
+
+    def merge_copy(c, dest):
+        return pltpu.make_async_remote_copy(
+            src_ref=block(piece(leaving_refs, c), dest),
+            dst_ref=block(piece(merge_refs, c), me - base),
+            send_sem=far_send.at[far_group(c)],
+            recv_sem=merge_recv.at[c],
+            device_id={"ep": lax.rem(dest + half, n)},
+            device_id_type=MESH,
+        )
+
+    def ends(peer):
+        return (peer // 2 == 0) | (peer // 2 == n // 2 - 1)
+
+    def merged_copy(c):
+        return pltpu.make_async_remote_copy(
+            src_ref=piece(merged_refs, c),
+            dst_ref=piece(merged_in_refs, c),
+            send_sem=merged_send.at[int(is_narrow(c))],
+            recv_sem=merged_recv.at[c],
+            device_id={"ep": partner},
+            device_id_type=MESH,
+        )
+
+    def blended(weights, values):
+        total = jnp.dot(weights[0], values, preferred_element_type=F32)
+        return total + jnp.dot(weights[1], values, preferred_element_type=F32)
+
+    def merge(c):
+        @when_passing
+        def _():
+            ready = piece(merge_refs, c).at[: (half - 1) * slot_count]
+            settle(ready, merge_recv.at[c]).wait_recv()
+            piece(merged_refs, c)[...] = blended(merge_blend, piece(merge_refs, c)[...]).astype(BF16)
+            merged_copy(c).start()
+
+    def results(c):
+        if c > 0:
+            weight_copy(3 + c, 1).wait_recv()
+            weight_copy(3 + c, 2).start()
+        weight_copy(3 + c, 2).wait_recv()
+        leaving = piece(leaving_refs, c)
+        leaving[...] = jnp.dot(
+            active_ref[...], piece(downs_refs, c)[...], preferred_element_type=F32
+        ).astype(BF16)
+
+        @when_passing
+        def _():
+            piece(merge_refs, c)[mine] = leaving[
+                pl.ds(pl.multiple_of(partner * slot_count, slot_count), slot_count)
+            ]
+
+        if relayed:
+
+            @each_far
+            def _(peer):
+                pl.when(ends(peer) & (peer != partner))(lambda: merge_copy(c, peer).start())
+
+        @each_far
+        def _(peer):
+            if relayed:
+                pl.when(jnp.logical_not(ends(peer)))(lambda: back_copy(c, peer, 1).start())
+            else:
+                back_copy(c, peer, 1).start()
+
+    def near(c):
+        each_near(lambda peer: back_copy(c, peer, 0).start())
+        piece(returned_refs, c)[here] = piece(leaving_refs, c)[here]
+
+    def collect(c):
+        returned = piece(returned_refs, c)
+        total = total_ref.at[:, : returned.shape[1]]
+        settle(returned.at[: (half - 1) * slot_count], back_recv.at[c, 0]).wait_recv()
+        total[...] = blended(blend_ref.at[base // half], returned[near_rows])
+
+        @when_middle
+        def _():
+            settle(returned.at[: half * slot_count], back_recv.at[c, 1]).wait_recv()
+            total[...] += blended(blend_ref.at[other // half], returned[far_rows])
+
+        @when_end
+        def _():
+            merged_copy(c).wait_recv()
+            total[...] += piece(merged_in_refs, c)[...].astype(F32)
+
+        routed_ref[:, columns(c)] = total[...].astype(BF16)
+
     diagonal = lax.rem(beside + quarters // 2, quarters)
 
     def piece_copy(i):
@@ -630,54 +688,72 @@
         total = partial_ref[3].astype(F32) + pieces_ref[1].astype(F32)
         mixed_ref[...] = (total + pieces_ref[2].astype(F32)).astype(BF16)
 
-    results(0)
-    direct(0)
-    results(1)
-    finish_mixer()
-    for c in range(2, pieces):
+    for c in range(pieces):
         results(c)
-        merge(c - 2)
-        direct(c - 1)
+        if c == 0:
+            near(0)
+        else:
+            when_middle(lambda: near(c))
+        if c == 4:
+            when_end(lambda: near(1))
+        if c == 1:
+            finish_mixer()
+        if c > 1:
+            merge(c - 2)
         if c == 2:
             project()
-        if c == 3:
+        if c == 4:
             cross()
-    collect(0)
-    collect(1)
+
+    def far_sent(group, blocks):
+        narrow, wide = leaving_refs
+        sent = (wide.at[: pieces - 3], narrow, wide.at[:1])[group]
+        settle(sent.at[:, : blocks * slot_count], far_send.at[group]).wait_send()
+
+    @when_end
+    def _():
+        far_sent(2, half)
+        for c in range(2, pieces):
+            near(c)
+
     merge(pieces - 2)
-    collect(2)
     merge(pieces - 1)
-    direct(pieces - 1)
-    for c in range(3, pieces - 1):
+    for c in range(pieces):
+        if c == pieces // 2:
+            gather_mixed()
         collect(c)
-    gather_mixed()
-    collect(pieces - 1)
 
     @when_end
     def _():
         rows_copy(0).wait_send()
         rows_copy(1).wait_send()
         settle(slots_ref.at[: (half - 1) * slot_count], slot_send).wait_send()
-        settle(leaving_ref.at[:, : (n - 1) * slot_count], back_send).wait_send()
+        for group in range(2):
+            far_sent(group, half)
 
     @when_middle
     def _():
-        blocks = n - 2 if relayed else n - 1
         settle(slots_ref.at[: (n - 1) * slot_count], slot_send).wait_send()
-        settle(leaving_ref.at[:, : blocks * slot_count], back_send).wait_send()
+        for group in range(3):
+            far_sent(group, half - 1 if relayed else half)
 
     @when_passing
     def _():
         settle(passed_ref.at[: (half - 1) * slot_count], pass_send).wait_send()
-        settle(merged_ref, merged_send).wait_send()
-
+        for kind in range(2):
+            settle(merged_refs[kind], merged_send.at[1 - kind]).wait_send()
+
+    for kind in range(2):
+        sent = leaving_refs[kind].at[:, : (half - 1) * slot_count]
+        settle(sent, near_send.at[1 - kind]).wait_send()
     settle(state_in.at[: n - 1], state_send).wait_send()
     for i in range(3):
         piece_copy(i).wait_send()
     for hop in range(3):
         settle(gates_ref.at[0], weight_send.at[0, hop]).wait_send()
         settle(ups_ref.at[0], weight_send.at[1, hop]).wait_send()
-        settle(downs_ref.at[:, :units], weight_send.at[2, hop]).wait_send()
+        for kind in range(2):
+            settle(downs_refs[kind].at[:, :units], weight_send.at[2 + kind, hop]).wait_send()
 
 
 def shards(
@@ -711,12 +787,19 @@
     depth = values.shape[1] // heads
     chunks = group_rows // CHUNK
     units = expert_down_matrix.shape[1]
-    span = width_model // PIECES
+    span = width_model // SPANS
     vmem = pl.BlockSpec(memory_space=pltpu.VMEM)
     anywhere = pl.BlockSpec(memory_space=pl.ANY)
     state = (heads, depth + DECAY_ROWS, channels)
     block = (group_rows, width)
     out = jax.ShapeDtypeStruct((row_count, width_model), BF16)
+
+    def narrow_and_wide(height):
+        return [
+            pltpu.VMEM((2, height, span), BF16),
+            pltpu.VMEM((PIECES - 2, height, 2 * span), BF16),
+        ]
+
     dma = pltpu.SemaphoreType.DMA
     return pl.pallas_call(
         functools.partial(fused_kernel, n, quarters),
@@ -743,15 +826,16 @@
             pltpu.VMEM((slot_total // 2, width_model), BF16),
             pltpu.VMEM((quarters,) + expert_gate_matrix.shape[1:], BF16),
             pltpu.VMEM((quarters,) + expert_up_matrix.shape[1:], BF16),
-            pltpu.VMEM((PIECES, quarters * units, span), BF16),
+            *narrow_and_wide(quarters * units),
             pltpu.VMEM((slot_total, quarters * units), F32),
             pltpu.VMEM((slot_total, quarters * units), BF16),
-            pltpu.VMEM((PIECES, slot_total, span), BF16),
-            pltpu.VMEM((PIECES, slot_total, span), BF16),
-            pltpu.VMEM((PIECES, slot_total // 2, span), BF16),
-            pltpu.VMEM((PIECES, row_count, span), BF16),
-            pltpu.VMEM((PIECES, row_count, span), BF16),
-            pltpu.VMEM((row_count, span), F32),
+            pltpu.VMEM((2, slot_total, units), F32),
+            *narrow_and_wide(slot_total),
+            *narrow_and_wide(slot_total),
+            *narrow_and_wide(slot_total // 2),
+            *narrow_and_wide(row_count),
+            *narrow_and_wide(row_count),
+            pltpu.VMEM((row_count, 2 * span), F32),
             pltpu.VMEM((heads, chunks, CHUNK, depth), F32),
             pltpu.VMEM((2, heads, chunks, CHUNK, channels), BF16),
             pltpu.VMEM((2, heads, chunks, depth, channels), F32),
@@ -762,19 +846,20 @@
             pltpu.VMEM((4, row_count, width_model), BF16),
             pltpu.VMEM((row_count, width_model), BF16),
             pltpu.VMEM((3, row_count, width_model), BF16),
-            dma((10,)),
+            dma((11,)),
             dma((2, 2)),
             dma(()),
             dma((PIECES,)),
-            dma(()),
+            dma((2,)),
             dma((PIECES,)),
             dma(()),
             dma((2,)),
             dma(()),
             dma(()),
-            dma((3, 3)),
-            dma((2 + PIECES, 3)),
-            dma(()),
+            dma((4, 3)),
+            dma((3 + PIECES, 3)),
+            dma((3,)),
+            dma((2,)),
             dma((PIECES, 2)),
             dma((3,)),
             dma((3,)),

time: 101 us -> 99.2 us (0.982)
  Pallas kernels: 98.1 us -> 96.7 us
    pallas_call x1, Pallas kernels: 98.1 us -> 96.7 us  [shards(): pl.pallas_call(functools.partial(fused_kernel, n, quarters), out_shape=(o...]
where the time goes in v4:
time: 99.2 us; the launch traced here: 99 us
  Pallas kernels  96.7 us (97%)
  local copies, waits for them, and re-layouts  1.59 us (2%)
    pallas_call x1, Pallas kernels, shards(): pl.pallas_call(functools.partial(fused_kernel, n, quarters), out_shape=(o...  96.7 us

profile of v4, /device:TPU:0, one launch (start us, length us, event | category | flops | bytes accessed | tf_op | source)
XLA Modules:
  0.0 99.0 jit_solution(1848594817617011474)
XLA Ops:
  0.6 96.7 %mix_and_route.1 = (bf16[128,2048]{1,0:T(8,128)(2,1)S(1)}, bf16[128,2048]{1,0:T(8,128)(2,1)S(1)}) custom-call(bf16[512,256]{1,0:T(8,128)(2,1)} %q_any.1, bf16[512,256]{1,0:T(8,128)(2,1)} %ff_any.1, bf16[512,256]{1,0:T(8,128)(2,1)} %fb_any.1, bf16[512,256]{1,0:T(8,128)(2,1)} %v_any.1, bf16[512,256]{1,0:T(8,128)(2,1)} %og_any.1, f32[1,256]{1,0:T(1,128)} %bitcast.10, ...), custom_call_target="tpu_custom_call" | custom-call | flops 40000000000 | bytes 31457280 | tf_op jit(solution)/shard_map/mix_and_route/pallas_call | solution.py:804
  97.4 0.8 copy.21
  98.2 0.8 copy.22

commit v5 on v4

--- a/solution.py
+++ b/solution.py
@@ -627,6 +627,7 @@
             def _(peer):
                 pl.when(ends(peer) & (peer != partner))(lambda: merge_copy(c, peer).start())
 
+    def far(c):
         @each_far
         def _(peer):
             if relayed:
@@ -688,8 +689,13 @@
         total = partial_ref[3].astype(F32) + pieces_ref[1].astype(F32)
         mixed_ref[...] = (total + pieces_ref[2].astype(F32)).astype(BF16)
 
+    early = 4
     for c in range(pieces):
         results(c)
+        if c < early or not relayed:
+            far(c)
+        else:
+            when_end(lambda: far(c))
         if c == 0:
             near(0)
         else:
@@ -698,7 +704,9 @@
             when_end(lambda: near(1))
         if c == 1:
             finish_mixer()
-        if c > 1:
+        if 0 < c < 3:
+            merge(c - 1)
+        if c > 3:
             merge(c - 2)
         if c == 2:
             project()
@@ -716,8 +724,13 @@
         for c in range(2, pieces):
             near(c)
 
+    for c in range(early, pieces - 3):
+        when_passing(lambda: far(c))
     merge(pieces - 2)
+    when_passing(lambda: far(pieces - 3))
     merge(pieces - 1)
+    for c in range(pieces - 2, pieces):
+        when_passing(lambda: far(c))
     for c in range(pieces):
         if c == pieces // 2:
             gather_mixed()

time: 99.2 us -> 97.5 us (0.983)
  Pallas kernels: 96.7 us -> 95.1 us
    pallas_call x1, Pallas kernels: 96.7 us -> 95.1 us  [shards(): pl.pallas_call(functools.partial(fused_kernel, n, quarters), out_shape=(o...]
where the time goes in v5:
time: 97.5 us; the launch traced here: 97.3 us
  Pallas kernels  95.1 us (98%)
  local copies, waits for them, and re-layouts  1.59 us (2%)
    pallas_call x1, Pallas kernels, shards(): pl.pallas_call(functools.partial(fused_kernel, n, quarters), out_shape=(o...  95.1 us

profile of v5, /device:TPU:0, one launch (start us, length us, event | category | flops | bytes accessed | tf_op | source)
XLA Modules:
  0.0 97.3 jit_solution(18181176312778465048)
XLA Ops:
  0.6 95.1 %mix_and_route.1 = (bf16[128,2048]{1,0:T(8,128)(2,1)S(1)}, bf16[128,2048]{1,0:T(8,128)(2,1)S(1)}) custom-call(bf16[512,256]{1,0:T(8,128)(2,1)} %q_any.1, bf16[512,256]{1,0:T(8,128)(2,1)} %ff_any.1, bf16[512,256]{1,0:T(8,128)(2,1)} %fb_any.1, bf16[512,256]{1,0:T(8,128)(2,1)} %v_any.1, bf16[512,256]{1,0:T(8,128)(2,1)} %og_any.1, f32[1,256]{1,0:T(1,128)} %bitcast.10, ...), custom_call_target="tpu_custom_call" | custom-call | flops 40000000000 | bytes 31457280 | tf_op jit(solution)/shard_map/mix_and_route/pallas_call | solution.py:817
  95.7 0.8 copy.21
  96.5 0.8 copy.22

commit v6 on v5

--- a/solution.py
+++ b/solution.py
@@ -83,20 +83,26 @@
     fb_any,
     v_any,
     og_any,
+    lbf_any,
+    lbb_any,
+    extra_any,
+    scale_any,
+    proj_any,
+    resid_any,
+    gain_any,
+    routes_any,
+    mix_any,
+    gate_any,
+    up_any,
+    down_any,
+    both_ref,
     lbf_ref,
     lbb_ref,
     extra_ref,
     scale_ref,
-    proj_any,
-    resid_any,
     gain_ref,
     routes_ref,
     mix_ref,
-    gate_any,
-    up_any,
-    down_any,
-    mixed_ref,
-    routed_ref,
     q_ref,
     ff_ref,
     fb_ref,
@@ -160,6 +166,7 @@
     piece_send,
     piece_recv,
 ):
+    mixed_ref, routed_ref = both_ref.at[0], both_ref.at[1]
     me = lax.axis_index("ep")
     place = lax.axis_index("tp")
     group_rows, width = q_ref.shape
@@ -246,7 +253,21 @@
         )
         for c in range(pieces)
     ]
-    for load in loads[:2] + down_loads + loads[2:]:
+    small_loads = [
+        pltpu.make_async_copy(source, target, load_sem.at[11 + i])
+        for i, (source, target) in enumerate(
+            (
+                (routes_any, routes_ref),
+                (mix_any, mix_ref),
+                (gain_any, gain_ref),
+                (extra_any, extra_ref),
+                (lbf_any, lbf_ref),
+                (lbb_any, lbb_ref),
+                (scale_any, scale_ref),
+            )
+        )
+    ]
+    for load in loads[:2] + small_loads + loads[2:3] + down_loads + loads[3:]:
         load.start()
 
     pl.semaphore_wait(pltpu.get_barrier_semaphore(), n + quarters - 2)
@@ -280,6 +301,9 @@
         pltpu.make_async_copy(own_part, own_part, load_sem.at[9 + kind]).wait()
     for c in range(pieces):
         weight_copy(3 + c, 1).start()
+
+    for load in small_loads:
+        load.wait()
 
     lanes = pl.ds(first_row, row_count)
     expert = lax.broadcasted_iota(jnp.int32, (n, row_count), 0)
@@ -814,16 +838,21 @@
         ]
 
     dma = pltpu.SemaphoreType.DMA
-    return pl.pallas_call(
+    both = pl.pallas_call(
         functools.partial(fused_kernel, n, quarters),
-        out_shape=(out, out),
-        in_specs=[anywhere] * 5
-        + [vmem] * 4
-        + [anywhere] * 2
-        + [vmem] * 3
-        + [anywhere] * 3,
-        out_specs=(vmem, vmem),
-        scratch_shapes=[pltpu.VMEM(block, BF16)] * 5
+        out_shape=jax.ShapeDtypeStruct((2, row_count, width_model), BF16),
+        in_specs=[anywhere] * 17,
+        out_specs=vmem,
+        scratch_shapes=[
+            pltpu.VMEM((1, width), F32),
+            pltpu.VMEM((1, width), F32),
+            pltpu.VMEM((heads, group_rows), F32),
+            pltpu.VMEM((1, width), F32),
+            pltpu.VMEM((1, width_model), F32),
+            pltpu.VMEM((TOPK, group_rows), jnp.int32),
+            pltpu.VMEM((TOPK, row_count), F32),
+        ]
+        + [pltpu.VMEM(block, BF16)] * 5
         + [
             pltpu.VMEM((width, width_model), BF16),
             pltpu.VMEM((row_count, width_model), BF16),
@@ -859,7 +888,7 @@
             pltpu.VMEM((4, row_count, width_model), BF16),
             pltpu.VMEM((row_count, width_model), BF16),
             pltpu.VMEM((3, row_count, width_model), BF16),
-            dma((11,)),
+            dma((18,)),
             dma((2, 2)),
             dma(()),
             dma((PIECES,)),
@@ -908,6 +937,7 @@
             )
         )
     )
+    return both[0], both[1]
 
 
 def solution(mesh):

time: 97.5 us -> 96.3 us (0.988)
    unnamed x2 -> x0, local copies, waits for them, and re-layouts: 1.59 us -> none
    squeeze x0 -> x1, local copies, waits for them, and re-layouts: none -> 1.08 us  [shards(): return (both[0], both[1])]
where the time goes in v6:
time: 96.3 us; the launch traced here: 96.1 us
  Pallas kernels  94.4 us (98%)
  local copies, waits for them, and re-layouts  1.08 us (1%)
    pallas_call x1, Pallas kernels, shards(): pl.pallas_call(functools.partial(fused_kernel, n, quarters), out_shape=ja...  94.4 us

profile of v6, /device:TPU:0, one launch (start us, length us, event | category | flops | bytes accessed | tf_op | source)
XLA Modules:
  0.0 96.1 jit_solution(128926273384596202)
XLA Ops:
  0.6 94.4 %mix_and_route.1 = bf16[2,128,2048]{2,1,0:T(8,128)(2,1)S(1)} custom-call(bf16[512,256]{1,0:T(8,128)(2,1)} %q_any.1, bf16[512,256]{1,0:T(8,128)(2,1)} %ff_any.1, bf16[512,256]{1,0:T(8,128)(2,1)} %fb_any.1, bf16[512,256]{1,0:T(8,128)(2,1)} %v_any.1, bf16[512,256]{1,0:T(8,128)(2,1)} %og_any.1, f32[1,256]{1,0:T(1,128)} %bitcast.14, f32[1,256]{1,0:T(1,128)} %bitcast.15, ...), custom_call_target="tpu_custom_call" | custom-call | flops 40000000000 | bytes 31457280 | tf_op jit(solution)/shard_map/mix_and_route/pallas_call | solution.py:841
  95.0 1.1 %slice_bitcast_fusion = (bf16[128,2048]{1,0:T(8,128)(2,1)}, bf16[128,2048]{1,0:T(8,128)(2,1)}) fusion(bf16[2,128,2048]{2,1,0:T(8,128)(2,1)S(1)} %mix_and_route.1), kind=kLoop, calls=%fused_computation | loop fusion | bytes 2097152 | tf_op jit(solution)/shard_map/squeeze | solution.py:940

commit v7 on v6

--- a/solution.py
+++ b/solution.py
@@ -724,8 +724,8 @@
             near(0)
         else:
             when_middle(lambda: near(c))
-        if c == 4:
-            when_end(lambda: near(1))
+        if c in (4, 7):
+            when_end(lambda: near(c // 3))
         if c == 1:
             finish_mixer()
         if 0 < c < 3:
@@ -745,7 +745,7 @@
     @when_end
     def _():
         far_sent(2, half)
-        for c in range(2, pieces):
+        for c in range(3, pieces):
             near(c)
 
     for c in range(early, pieces - 3):

time: 96.3 us -> 96.3 us (level)
  no operation moved by 1% of the time
where the time goes in v7:
time: 96.3 us; the launch traced here: 96.1 us
  Pallas kernels  94.4 us (98%)
  local copies, waits for them, and re-layouts  1.08 us (1%)
    pallas_call x1, Pallas kernels, shards(): pl.pallas_call(functools.partial(fused_kernel, n, quarters), out_shape=ja...  94.4 us

profile of v7, /device:TPU:0, one launch (start us, length us, event | category | flops | bytes accessed | tf_op | source)
XLA Modules:
  0.0 96.1 jit_solution(4639871921624633938)
XLA Ops:
  0.6 94.4 %mix_and_route.1 = bf16[2,128,2048]{2,1,0:T(8,128)(2,1)S(1)} custom-call(bf16[512,256]{1,0:T(8,128)(2,1)} %q_any.1, bf16[512,256]{1,0:T(8,128)(2,1)} %ff_any.1, bf16[512,256]{1,0:T(8,128)(2,1)} %fb_any.1, bf16[512,256]{1,0:T(8,128)(2,1)} %v_any.1, bf16[512,256]{1,0:T(8,128)(2,1)} %og_any.1, f32[1,256]{1,0:T(1,128)} %bitcast.14, f32[1,256]{1,0:T(1,128)} %bitcast.15, ...), custom_call_target="tpu_custom_call" | custom-call | flops 40000000000 | bytes 31457280 | tf_op jit(solution)/shard_map/mix_and_route/pallas_call | solution.py:841
  95.0 1.1 %slice_bitcast_fusion = (bf16[128,2048]{1,0:T(8,128)(2,1)}, bf16[128,2048]{1,0:T(8,128)(2,1)}) fusion(bf16[2,128,2048]{2,1,0:T(8,128)(2,1)S(1)} %mix_and_route.1), kind=kLoop, calls=%fused_computation | loop fusion | bytes 2097152 | tf_op jit(solution)/shard_map/squeeze | solution.py:940
